TPU v7x, 256 devices: a whole 4x4x8 slice. The times are simulated.
256 devices in a mesh: ep: 64 (over z, y, core), tp: 4 (over x).
Axes of the slice: x: 4, y: 4, z: 8, core: 2. Of those that a mesh axis runs over, the one named last changes fastest.
Arguments:
- queries: bfloat16 [8192, 512], P('ep', 'tp'), may hold values from -8 to 8
- key_cache: bfloat16 [4, 64, 8192], P('tp', None, 'ep'), may hold values from -4.5 to 4.5
- value_cache: bfloat16 [4, 64, 8192], P('tp', None, 'ep'), may hold values from -6 to 6
- cum_gate: float32 [4, 8192], P('tp'), may hold values from -2048 to 0, as said below
- out_weight: bfloat16 [512, 2048], replicated, may hold values from -1 to 1
- routed_input: bfloat16 [16384, 2048], P('ep'), may hold values from -6 to 6
- norm_gain: bfloat16 [2048], replicated, may hold values from 0.099609375 to 1.8984375
- routes: int32 [16384, 2], P('ep'), may hold values from 0 to 63, all different within a row; in each aligned block of 64 rows (0 to 63, 64 to 127, ...) at most 3 rows name the same one
- route_weight: float32 [16384, 2], P('ep'), may hold values from 0.2 to 1
- expert_gate: bfloat16 [64, 2048, 1024], P('ep', None, 'tp'), may hold values from -0.125 to 0.125
- expert_up: bfloat16 [64, 2048, 1024], P('ep', None, 'tp'), may hold values from -0.125 to 0.125
- expert_down: bfloat16 [64, 1024, 2048], P('ep', 'tp'), may hold values from -0.1875 to 0.1875
Outputs:
- mixed_out: bfloat16 [8192, 2048], P(('ep', 'tp'))
- expert_out: bfloat16 [16384, 2048], P(('ep', 'tp'))
Inputs may be any that keep to these rules, and one draw needn't show every extreme that they name: `cum_gate`: Non-increasing along positions in every head. `routes`: each row names 2 different experts. In each aligned block of 64 rows (the rows of one device) no expert is named by more than 3 rows, a bound that some block reaches.
All inputs are finite; a program needn't handle non-finite values.
Results may differ from a plain program's by a relative error of at most 0.012.
Values may be sent and summed in bfloat16 or wider, within the bound.
A program may use at most 64 MiB of HBM per device.

v0:
```python
import jax
import jax.numpy as jnp
from jax import lax
from jax.sharding import PartitionSpec as P


def side_by_side(arrays, axis, dim, along):
    both = jnp.concatenate(arrays, axis=along)
    out, at, gathered = (lax.all_gather(both, axis, axis=dim, tiled=True), 0, [])
    for a in arrays:
        gathered.append(lax.slice_in_dim(out, at, at + a.shape[along], axis=along))
        at += a.shape[along]
    return tuple(gathered)


def joined_along(parts, dim):
    lengths = list(parts.shape[1:])
    lengths[dim] *= parts.shape[0]
    return jnp.moveaxis(parts, 0, dim).reshape(lengths)


def copy_for_each(x, axis):
    count = lax.axis_size(axis)
    return lax.all_to_all(jnp.broadcast_to(x[None], (count, *x.shape)), axis, 0, 0, tiled=True)


def gather_directly(x, axis, dim):
    return joined_along(copy_for_each(x, axis), dim)


def in_blocks(x, dim, count):
    before, after = (x.shape[:dim], x.shape[dim + 1 :])
    return jnp.moveaxis(x.reshape(*before, count, -1, *after), dim, 0)


def sum_at_owner(x, axis, dim):
    count = lax.axis_size(axis)
    parts = lax.all_to_all(in_blocks(x, dim, count), axis, 0, 0, tiled=True)
    return jnp.sum(parts.astype(jnp.float32), axis=0)


def slot_chooser(route_rows, expert_count, capacity):
    token_rows, top_count = route_rows.shape
    flat = route_rows.reshape(token_rows * top_count)
    same = (flat[:, None] == jnp.arange(expert_count, dtype=jnp.int32)[None, :]).astype(jnp.int32)
    earlier = jnp.cumsum(same, axis=0) - same
    rank = jnp.sum(earlier * same, axis=1)
    slot = flat * capacity + rank
    chosen = slot[:, None] == jnp.arange(expert_count * capacity, dtype=jnp.int32)[None, :]
    return chosen.astype(jnp.bfloat16).reshape(token_rows, top_count, expert_count * capacity)


def rms_rows(source, norm_gain):
    widened = source.astype(jnp.float32)
    scale = lax.rsqrt(jnp.mean(widened * widened, axis=-1, keepdims=True) + 1e-06)
    return (widened * scale * norm_gain.astype(jnp.float32)).astype(jnp.bfloat16)


def mixer_half(queries, key_cache, value_cache, cum_gate, out_weight):
    seq_rows = queries.shape[0]
    local_heads = key_cache.shape[0]
    head_size = key_cache.shape[1]
    group = queries.shape[1] // (local_heads * head_size)
    own_start = lax.axis_index("ep") * seq_rows
    query_heads = queries.reshape(seq_rows, local_heads, group, head_size)
    query_pos = own_start + jnp.arange(seq_rows, dtype=jnp.int32)
    gate_query = lax.dynamic_slice_in_dim(cum_gate, own_start, seq_rows, 1)
    gate_rows = jnp.transpose(gate_query)[:, :, None, None]
    scale = head_size ** (-0.5)
    best_start = jnp.full((seq_rows, local_heads, group), -jnp.inf, jnp.float32)
    total_start = jnp.zeros((seq_rows, local_heads, group), jnp.float32)
    summed_start = jnp.zeros((seq_rows, local_heads * group * head_size), jnp.float32)
    pieces = side_by_side((key_cache, value_cache), "ep", 2, 0)

    def update(state):
        best, total, summed = state
        key_piece, value_piece = pieces
        width = key_piece.shape[2]
        scores = (
            jnp.einsum("thgd,hds->thgs", query_heads, key_piece, preferred_element_type=jnp.float32)
            * scale
        )
        scores = scores + gate_rows - cum_gate[None, :, None, :]
        key_pos = jnp.arange(width, dtype=jnp.int32)
        allowed = key_pos[None, :] <= query_pos[:, None]
        scores = jnp.where(allowed[:, None, None, :], scores, -jnp.inf)
        new_best = jnp.max(scores, axis=-1)
        factor = jnp.exp(best - new_best)
        weights = jnp.exp(scores - new_best[..., None])
        new_total = total * factor + jnp.sum(weights, axis=-1)
        product = jnp.einsum(
            "thgs,hds->thgd",
            weights.astype(jnp.bfloat16),
            value_piece,
            preferred_element_type=jnp.float32,
        )
        new_summed = summed.reshape(product.shape) * factor[..., None] + product
        return (new_best, new_total, new_summed.reshape(seq_rows, local_heads * group * head_size))

    best, total, summed = lax.cond(
        jnp.int32(0) <= own_start,
        update,
        lambda state: state,
        (best_start, total_start, summed_start),
    )
    attended = summed.reshape(seq_rows, local_heads, group, head_size) / total[..., None]
    attended = attended.astype(jnp.bfloat16).reshape(seq_rows, local_heads * group * head_size)
    by_position = lax.all_to_all(attended, "tp", split_axis=0, concat_axis=1, tiled=True)
    return jnp.dot(by_position, out_weight, preferred_element_type=jnp.float32).astype(jnp.bfloat16)


def expert_half(routed_input, norm_gain, routes, route_weight, expert_gate, expert_up, expert_down):
    group_size = lax.axis_size("tp")
    ep_size = lax.axis_size("ep")
    tp_index = lax.axis_index("tp")
    seq_rows, width = routed_input.shape
    own_rows = seq_rows // group_size
    local_experts = expert_gate.shape[0]
    expert_count = local_experts * ep_size
    top_count = routes.shape[1]
    capacity = max(2, own_rows * top_count * 3 // (2 * expert_count))
    per_device = local_experts * capacity

    def hidden_units(received):
        blocks = received.shape[0]
        divide_point = received.reshape(blocks, ep_size, local_experts, capacity, width)
        gate = jnp.einsum(
            "abecd,edf->abecf", divide_point, expert_gate, preferred_element_type=jnp.float32
        )
        upper = jnp.einsum(
            "abecd,edf->abecf", divide_point, expert_up, preferred_element_type=jnp.float32
        )
        return (jax.nn.silu(gate) * upper).astype(jnp.bfloat16)

    mine = lax.dynamic_slice_in_dim(routed_input, tp_index * own_rows, own_rows, 0)
    own_routes = lax.dynamic_slice_in_dim(routes, tp_index * own_rows, own_rows, 0)
    chooser = slot_chooser(own_routes, expert_count, capacity)
    normed = rms_rows(mine, norm_gain)
    outgoing = jnp.einsum("tks,td->sd", chooser, normed, preferred_element_type=jnp.float32).astype(
        jnp.bfloat16
    )
    arrived = lax.all_to_all(
        outgoing.reshape(1, ep_size, per_device, width),
        "ep",
        split_axis=1,
        concat_axis=1,
        tiled=True,
    )
    hidden = (lambda piece, start: hidden_units(piece))(
        gather_directly(arrived, "tp", 0), jnp.int32(0)
    )
    partial_value = jnp.einsum(
        "abecf,efd->abecd", hidden, expert_down, preferred_element_type=jnp.float32
    )
    rounded = lax.optimization_barrier(partial_value.astype(jnp.bfloat16)).astype(jnp.float32)
    summed = sum_at_owner(
        rounded.reshape(1 * lax.axis_size("tp"), ep_size, per_device, width).astype(jnp.bfloat16),
        "tp",
        0,
    )
    returned = lax.all_to_all(
        summed.astype(jnp.bfloat16), "ep", split_axis=1, concat_axis=1, tiled=True
    )
    picked = jnp.einsum(
        "tks,sd->tkd",
        chooser,
        returned.reshape(ep_size * per_device, width),
        preferred_element_type=jnp.float32,
    )
    own_weight = lax.dynamic_slice_in_dim(route_weight, tp_index * own_rows, own_rows, 0)
    return jnp.sum(own_weight[:, :, None] * picked, axis=1).astype(jnp.bfloat16)


def body(
    queries,
    key_cache,
    value_cache,
    cum_gate,
    out_weight,
    routed_input,
    norm_gain,
    routes,
    route_weight,
    expert_gate,
    expert_up,
    expert_down,
):
    mixed_out = mixer_half(queries, key_cache, value_cache, cum_gate, out_weight)
    expert_out = expert_half(
        routed_input, norm_gain, routes, route_weight, expert_gate, expert_up, expert_down
    )
    return (mixed_out, expert_out)


def solution(mesh):
    return jax.shard_map(
        body,
        mesh=mesh,
        in_specs=(
            P("ep", "tp"),
            P("tp", None, "ep"),
            P("tp", None, "ep"),
            P("tp", None),
            P(),
            P("ep", None),
            P(),
            P("ep", None),
            P("ep", None),
            P("ep", None, "tp"),
            P("ep", None, "tp"),
            P("ep", "tp", None),
        ),
        out_specs=(P(("ep", "tp"), None), P(("ep", "tp"), None)),
        check_vma=False,
    )
```

profile of v0, /device:TPU:1, one launch (start us, length us, event | category | flops | bytes accessed | tf_op | source)
XLA Modules:
  0.0 209.8 jit_solution(6337569638874446934)
XLA Ops:
  7.2 0.0 copy-start
  7.2 0.9 constant_dynamic-slice_fusion
  8.1 0.1 copy.63
  8.2 0.1 eq.51
  8.3 0.1 fusion.62
  8.4 0.2 reduce_window_sum.11
  8.6 0.2 select_reduce_fusion
  8.8 0.1 reduce_sum.62
  8.9 0.1 copy.64
  9.0 0.8 multiply_add_fusion
  9.8 0.1 convert_reduce_fusion
  9.9 0.7 convert_element_type.77
  10.5 1.1 fusion.49
  11.7 2.3 %convolution_convert_fusion.1 = bf16[192,2048]{1,0:T(8,128)(2,1)} fusion(bf16[64,192]{1,0:T(8,128)(2,1)S(1)} %convert_reduce_fusion, f32[2048]{0:T(1024)S(1)} %convert_element_type.77, f32[64]{0:T(128)S(1)} %add_rsqrt_fusion, bf16[256,2048]{1,0:T(8,128)(2,1)} %param.19, s32[]{:T(128)S(6)} %select_n.15), kind=kOutput, calls=%fused_computation.30 | convolution fusion | flops 50855936 | bytes 1081604 | tf_op jit(solution)/shard_map/tks,td->sd/dot_general | solution.py:139
  13.9 2.4 %reshape.234 = bf16[1,64,3,2048]{3,2,1,0:T(4,128)(2,1)S(1)} reshape(bf16[192,2048]{1,0:T(8,128)(2,1)} %convolution_convert_fusion.1) | data formatting | bytes 1572864 | tf_op jit(solution)/shard_map/reshape | solution.py:143
  16.4 41.1 %all_to_all.39 = bf16[1,64,3,2048]{3,2,0,1:T(4,128)(2,1)S(1)} all-to-all(bf16[1,64,3,2048]{3,2,0,1:T(4,128)(2,1)S(1)} %bitcast.147), channel_id=1, replica_groups=mesh['ep'=64,'tp'=4] {'ep'}, dimensions={1} | all-to-all | bytes 1572864 | tf_op jit(solution)/shard_map/all_to_all | solution.py:142
  57.5 0.6 copy.66
  58.1 0.0 copy-start.3
  58.1 0.0 copy-start.4
  58.1 2.1 broadcast_in_dim.37
  60.2 4.6 %all-to-all-start.2 = ((bf16[4,1,64,3,2048]{4,2,3,1,0:T(8,128)(2,1)}), bf16[4,1,64,3,2048]{4,2,3,1,0:T(8,128)(2,1)}, u32[]{:S(2)}, u32[]{:S(2)}) async-start(bf16[4,1,64,3,2048]{4,2,3,1,0:T(8,128)(2,1)} %broadcast_in_dim.37), calls=%async_computation.2 | async-start | bytes 6291456 | tf_op jit(solution)/shard_map/all_to_all | solution.py:24
  64.8 0.0 all-gather.2.cloned.1.call-start
  64.9 0.6 pad_maximum_fusion
  65.5 0.0 all-gather.2.cloned.1.call-update
  65.5 35.8 %all-to-all-done.2 = bf16[4,1,64,3,2048]{4,2,3,1,0:T(8,128)(2,1)} async-done(((bf16[4,1,64,3,2048]{4,2,3,1,0:T(8,128)(2,1)}), bf16[4,1,64,3,2048]{4,2,3,1,0:T(8,128)(2,1)}, u32[]{:S(2)}, u32[]{:S(2)}) %all-to-all-start.2) | async-done | bytes 3145760 | tf_op jit(solution)/shard_map/all_to_all | solution.py:24
  101.4 3.8 %fusion.26 = f32[4,64,1,3,256]{4,1,3,0,2:T(8,128)} fusion(bf16[4,1,64,3,2048]{4,2,3,1,0:T(8,128)(2,1)} %all-to-all-done.2, bf16[1,2048,256]{2,1,0:T(8,128)(2,1)S(1)} %copy-done.6), kind=kOutput, calls=%fused_computation.33 | convolution fusion | flops 805306368 | bytes 4980736 | tf_op jit(solution)/shard_map/abecd,edf->abecf/dot_general | solution.py:127
  105.2 7.7 %fusion.25 = bf16[4,64,1,3,2048]{4,1,3,0,2:T(8,128)(2,1)} fusion(bf16[1,256,2048]{2,1,0:T(8,128)(2,1)} %param.25, bf16[4,1,64,3,2048]{4,2,3,1,0:T(8,128)(2,1)} %all-to-all-done.2, bf16[1,2048,256]{2,1,0:T(8,128)(2,1)} %param.24, f32[4,64,1,3,256]{4,1,3,0,2:T(8,128)} %fusion.26), kind=kOutput, calls=%fused_computation.29 | convolution fusion | flops 1613365248 | bytes 9175040 | tf_op jit(solution)/shard_map/abecf,efd->abecd/dot_general | solution.py:152
  112.9 4.8 %all-to-all-start.3 = ((bf16[4,1,64,3,2048]{4,2,3,1,0:T(8,128)(2,1)}), bf16[4,1,64,3,2048]{4,2,3,1,0:T(8,128)(2,1)}, u32[]{:S(2)}, u32[]{:S(2)}) async-start(bf16[4,1,64,3,2048]{4,2,3,1,0:T(8,128)(2,1)} %bitcast.149), calls=%async_computation.3 | async-start | bytes 6291456 | tf_op jit(solution)/shard_map/all_to_all | solution.py:38
  117.7 21.0 %all-gather.2.cloned.1.call-done = bf16[2,64,8192]{2,1,0:T(8,128)(2,1)} async-done(((bf16[2,64,128]{2,1,0:T(8,128)(2,1)}), bf16[2,64,8192]{2,1,0:T(8,128)(2,1)}) %all-gather.2.cloned.1.call-update) | async-done | bytes 2097168 | tf_op jit(solution)/shard_map/all_gather | solution.py:9
  138.7 7.7 %conditional.1 = (f32[128,1,2]{0,2,1:T(2,128)S(1)}, f32[128,128]{0,1:T(8,128)S(1)}) conditional(s32[]{:T(128)} %convert_element_type.70, () %tuple.19, (s32[]{:T(128)}, s32[128]{0:T(128)S(1)}, bf16[2,64,8192]{2,1,0:T(8,128)(2,1)}, bf16[128,128]{1,0:T(8,128)(2,1)S(1)}, f32[1,8192]{1,0:T(1,128)S(1)}) %tuple.35), branch_computations={%region_0.0_spmd, %region_1.4_spmd} | conditional | flops 556810624 | bytes 37957720 | solution.py:100
  138.7 0.1 dynamic-slice_bitcast_fusion
  138.7 0.1 copy.60
  138.9 0.7 iota_compare_fusion
  139.6 3.8 %fusion.67 = (f32[128,2]{0,1:T(2,128)S(1)}, f32[128,1,2,8192]{0,3,2,1:T(8,128)S(1)}) fusion(f32[8192]{0:T(1024)S(1)} %bitcast.154, f32[128]{0:T(128)S(1)} %dynamic-slice_bitcast_fusion, bf16[128,2,64]{0,2,1:T(8,128)(2,1)S(1)} %bitcast.152, bf16[2,64,8192]{2,1,0:T(8,128)(2,1)} %get-tuple-element.52, pred[128,8192]{0,1:T(8,128)(4,1)S(1)} %iota_compare_fusion), kind=kOutput, calls=%fused_computation.71 | convolution fusion | flops 278920960 | bytes 10552832 | tf_op jit(solution)/shard_map/cond/branch_1_fun/thgd,hds->thgs/dot_general | solution.py:80
  143.4 1.1 fusion.6
  144.5 0.5 copy-done.1
  145.0 1.4 fusion.14
  146.4 0.7 copy.61
  147.2 6.2 %all-to-all-done.3 = bf16[4,1,64,3,2048]{4,2,3,1,0:T(8,128)(2,1)} async-done(((bf16[4,1,64,3,2048]{4,2,3,1,0:T(8,128)(2,1)}), bf16[4,1,64,3,2048]{4,2,3,1,0:T(8,128)(2,1)}, u32[]{:S(2)}, u32[]{:S(2)}) %all-to-all-start.3) | async-done | bytes 3145760 | tf_op jit(solution)/shard_map/all_to_all | solution.py:38
  153.4 3.4 %all-to-all-start = ((bf16[4,32,128]{2,1,0:T(8,128)(2,1)}), bf16[4,32,128]{2,1,0:T(8,128)(2,1)S(1)}, u32[]{:S(2)}, u32[]{:S(2)}) async-start(bf16[4,32,128]{2,1,0:T(8,128)(2,1)} %bitcast.17), calls=%async_computation | async-start | bytes 65536 | tf_op jit(solution)/shard_map/all_to_all | solution.py:108
  156.9 2.5 %bitcast_reduce_fusion = bf16[64,3,2048]{2,0,1:T(8,128)(2,1)S(1)} fusion(bf16[4,1,64,3,2048]{4,2,3,1,0:T(8,128)(2,1)} %all-to-all-done.3), kind=kLoop, calls=%fused_computation.24 | loop fusion | flops 1179648 | bytes 3932160 | tf_op jit(solution)/shard_map/reduce_sum | solution.py:39
  159.3 1.7 copy.69
  161.0 10.1 %all-to-all-start.4 = ((bf16[1,64,3,2048]{3,2,0,1:T(4,128)(2,1)}), bf16[1,64,3,2048]{3,2,0,1:T(4,128)(2,1)S(1)}, u32[]{:S(2)}, u32[]{:S(2)}) async-start(bf16[1,64,3,2048]{3,2,0,1:T(4,128)(2,1)} %copy.69), calls=%async_computation.4 | async-start | bytes 2097152 | tf_op jit(solution)/shard_map/all_to_all | solution.py:161
  171.1 0.1 constant_dynamic-slice_fusion.1
  171.2 1.1 convolution_convert_fusion.2
  172.3 26.9 %all-to-all-done.4 = bf16[1,64,3,2048]{3,2,0,1:T(4,128)(2,1)S(1)} async-done(((bf16[1,64,3,2048]{3,2,0,1:T(4,128)(2,1)}), bf16[1,64,3,2048]{3,2,0,1:T(4,128)(2,1)S(1)}, u32[]{:S(2)}, u32[]{:S(2)}) %all-to-all-start.4) | async-done | bytes 786464 | tf_op jit(solution)/shard_map/all_to_all | solution.py:161
  199.3 1.4 reshape.246
  200.7 2.3 %fusion.35 = bf16[64,2048]{1,0:T(8,128)(2,1)} fusion(bf16[192,2048,1]{1,0,2:T(8,128)(2,1)} %reshape.246, f32[64,2]{0,1:T(2,128)S(1)} %constant_dynamic-slice_fusion.1, s32[64,2]{0,1:T(2,128)S(1)} %multiply_add_fusion), kind=kOutput, calls=%fused_computation.36 | convolution fusion | flops 101081088 | bytes 1049600 | tf_op jit(solution)/shard_map/tks,sd->tkd/dot_general | solution.py:164
  (18 shorter events, 0.1 us)
Async XLA Ops:
  7.2 164.0 %copy-start = (bf16[512,2048]{1,0:T(8,128)(2,1)S(1)}, bf16[512,2048]{1,0:T(8,128)(2,1)}, u32[]{:S(2)}) copy-start(bf16[512,2048]{1,0:T(8,128)(2,1)} %param.18) | copy-start | bytes 6291460
  58.1 6.8 %copy-start.3 = (bf16[1,64,128]{2,1,0:T(8,128)(2,1)S(1)}, bf16[1,64,128]{2,1,0:T(8,128)(2,1)}, u32[]{:S(2)}) copy-start(bf16[1,64,128]{2,1,0:T(8,128)(2,1)} %param.16) | copy-start | bytes 49156
  58.1 6.8 %copy-start.4 = (bf16[1,64,128]{2,1,0:T(8,128)(2,1)S(1)}, bf16[1,64,128]{2,1,0:T(8,128)(2,1)}, u32[]{:S(2)}) copy-start(bf16[1,64,128]{2,1,0:T(8,128)(2,1)} %param.15) | copy-start | bytes 49156
  58.1 43.3 %copy-start.6 = (bf16[1,2048,256]{2,1,0:T(8,128)(2,1)S(1)}, bf16[1,2048,256]{2,1,0:T(8,128)(2,1)}, u32[]{:S(2)}) copy-start(bf16[1,2048,256]{2,1,0:T(8,128)(2,1)} %param.23) | copy-start | bytes 3145732
  60.2 41.2 %all-to-all-start.2 = ((bf16[4,1,64,3,2048]{4,2,3,1,0:T(8,128)(2,1)}), bf16[4,1,64,3,2048]{4,2,3,1,0:T(8,128)(2,1)}, u32[]{:S(2)}, u32[]{:S(2)}) async-start(bf16[4,1,64,3,2048]{4,2,3,1,0:T(8,128)(2,1)} %broadcast_in_dim.37), calls=%async_computation.2 | async-start | bytes 6291456 | tf_op jit(solution)/shard_map/all_to_all | solution.py:24
  64.8 73.9 %all-gather.2.cloned.1.call-start = ((), (), s32[]{:S(2)}) async-start(), calls=%async_computation.5 | async-start | bytes 2129920 | tf_op jit(solution)/shard_map/all_gather | solution.py:9
  112.9 25.8 %copy-start.2 = (bf16[128,128]{1,0:T(8,128)(2,1)S(1)}, bf16[128,128]{1,0:T(8,128)(2,1)}, u32[]{:S(2)}) copy-start(bf16[128,128]{1,0:T(8,128)(2,1)} %param.14) | copy-start | bytes 98308
  112.9 25.8 %copy-start.7 = (f32[1,8192]{1,0:T(1,128)S(1)}, f32[1,8192]{1,0:T(1,128)}, u32[]{:S(2)}) copy-start(f32[1,8192]{1,0:T(1,128)} %param.17) | copy-start | bytes 98308
  112.9 40.5 %all-to-all-start.3 = ((bf16[4,1,64,3,2048]{4,2,3,1,0:T(8,128)(2,1)}), bf16[4,1,64,3,2048]{4,2,3,1,0:T(8,128)(2,1)}, u32[]{:S(2)}, u32[]{:S(2)}) async-start(bf16[4,1,64,3,2048]{4,2,3,1,0:T(8,128)(2,1)} %bitcast.149), calls=%async_computation.3 | async-start | bytes 6291456 | tf_op jit(solution)/shard_map/all_to_all | solution.py:38
  143.4 1.6 copy-start.1
  146.4 24.7 %copy-start.5 = (f32[256,2]{0,1:T(2,128)S(1)}, f32[256,2]{0,1:T(2,128)}, u32[]{:S(2)}) copy-start(f32[256,2]{0,1:T(2,128)} %param.22) | copy-start | bytes 6148
  153.4 7.6 %all-to-all-start = ((bf16[4,32,128]{2,1,0:T(8,128)(2,1)}), bf16[4,32,128]{2,1,0:T(8,128)(2,1)S(1)}, u32[]{:S(2)}, u32[]{:S(2)}) async-start(bf16[4,32,128]{2,1,0:T(8,128)(2,1)} %bitcast.17), calls=%async_computation | async-start | bytes 65536 | tf_op jit(solution)/shard_map/all_to_all | solution.py:108
  161.0 38.3 %all-to-all-start.4 = ((bf16[1,64,3,2048]{3,2,0,1:T(4,128)(2,1)}), bf16[1,64,3,2048]{3,2,0,1:T(4,128)(2,1)S(1)}, u32[]{:S(2)}, u32[]{:S(2)}) async-start(bf16[1,64,3,2048]{3,2,0,1:T(4,128)(2,1)} %copy.69), calls=%async_computation.4 | async-start | bytes 2097152 | tf_op jit(solution)/shard_map/all_to_all | solution.py:161
Sparse Core Ops, SparseCore 0:
  68.8 69.7 all-gather.1
where the time goes:
time: 211 us; the launch traced here: 210 us
  waiting for transfers between devices  90 us (43%)
  blocking collectives  41.1 us (19%)
  starting transfers between devices  23 us (11%)
  matrix products  22.4 us (11%)
  between operations  14.2 us (7%)
  local copies, waits for them, and re-layouts  11 us (5%)
  other arithmetic  7.98 us (4%)
    all_to_all x1, blocking collectives, expert_half(): lax.all_to_all(outgoing.reshape(1, ep_size, per_device, width), 'ep', spl...  41.1 us
    all_to_all x1, waiting for transfers between devices, copy_for_each(): lax.all_to_all(jnp.broadcast_to(x[None], (count, *x.shape)), axis, 0, 0,...  35.8 us
    all_to_all x1, waiting for transfers between devices, expert_half(): lax.all_to_all(summed.astype(jnp.bfloat16), 'ep', split_axis=1, concat_ax...  26.9 us
    all_gather x1, waiting for transfers between devices, side_by_side(): lax.all_gather(both, axis, axis=dim, tiled=True)  21 us
    all_to_all x1, starting transfers between devices, expert_half(): lax.all_to_all(summed.astype(jnp.bfloat16), 'ep', split_axis=1, concat_ax...  10.1 us
    dot_general x1, matrix products, expert_half(): jnp.einsum('abecf,efd->abecd', hidden, expert_down, preferred_element_typ...  7.72 us
    all_to_all x1, waiting for transfers between devices, sum_at_owner(): parts = lax.all_to_all(in_blocks(x, dim, count), axis, 0, 0, tiled=True)  6.25 us
    all_to_all x1, starting transfers between devices, sum_at_owner(): parts = lax.all_to_all(in_blocks(x, dim, count), axis, 0, 0, tiled=True)  4.77 us
  transfers between devices with their start and end apart: 5, of which 4 were waited for; matrix products, arithmetic and copies ran while one was open for 12% of the time, Pallas kernels for 0%

commit v1 on v0

v1 whole, which is shorter than its diff:
```python
import functools

import jax
import jax.numpy as jnp
from jax import lax
from jax.experimental import pallas as pl
from jax.experimental.pallas import tpu as pltpu
from jax.sharding import PartitionSpec as P

MESH = pl.DeviceIdType.MESH
BF = jnp.bfloat16
F32 = jnp.float32

D = 2048
ROWS = 64
CAP = 3
NT = 4
NZ = 8
NYC = 8
NE = NZ * NYC
SL = NE * CAP
TR = D // 128
CH = CAP * TR
QR = NYC * CH
ALL = NE * CH
NP = NZ // 2
PT = 2 * NYC * CAP
HID = 256
DZ = (0, 1, 7, 2, 6, 3, 5, 4)


def permutation():
    a = lax.broadcasted_iota(jnp.int32, (256, 256), 0)
    b = lax.broadcasted_iota(jnp.int32, (256, 256), 1)
    hit = ((a & 15) == (b >> 4)) & ((a >> 4) == (b & 15))
    return hit.astype(F32).astype(BF)


def mm(a, b):
    return jnp.dot(a, b, preferred_element_type=F32)


def rows_to_tiles(perm, src, row, dst, at):
    z = jnp.concatenate([src[row : row + 16, 128 * i : 128 * i + 128] for i in range(TR)], axis=0)
    dst[at : at + 256, :] = mm(perm, z).astype(BF)


def moe_kernel(
    x_hbm, routes_ref, rw_ref, gain_ref, wg_hbm, wu_hbm, wd_hbm,
    out_ref,
    xin, obuf, pick, send, recv, wg, wu, wd, xb, part, rs1, rss, rsd, sumb, tot, ret, back, resb,
    ld_sem, as_sem, a_sem, xs_sem, gl_sem, gr_sem, g2_sem, rr_sem, r1_sem, rss_sem, rsd_sem, bs_sem, b_sem,
):
    t = lax.axis_index("tp")
    me = lax.axis_index("ep")
    z = me // NYC
    yc = me % NYC
    right = (t + 1) % NT
    left = (t + 3) % NT
    opp = (t + 2) % NT

    loads = [
        pltpu.make_async_copy(x_hbm.at[pl.ds(pl.multiple_of(t * ROWS, ROWS), ROWS), :], xin, ld_sem.at[0]),
        pltpu.make_async_copy(wg_hbm, wg, ld_sem.at[1]),
        pltpu.make_async_copy(wu_hbm, wu, ld_sem.at[2]),
        pltpu.make_async_copy(wd_hbm, wd, ld_sem.at[3]),
    ]
    for c in loads:
        c.start()

    barrier = pltpu.get_barrier_semaphore()

    def greet(k, _):
        pl.semaphore_signal(barrier, inc=1, device_id=((me + k) % NE, t), device_id_type=MESH)
        return 0

    lax.fori_loop(1, NE, greet, 0)
    for x in (right, left):
        pl.semaphore_signal(barrier, inc=1, device_id=(me, x), device_id_type=MESH)

    perm = permutation()

    own = pl.ds(pl.multiple_of(t * ROWS, ROWS), ROWS)
    r = routes_ref[own, :]
    r0 = r[:, 0:1]
    r1 = r[:, 1:2]
    lane = lax.broadcasted_iota(jnp.int32, (ROWS, NE), 1)
    s0 = jnp.where(r0 == lane, 1.0, 0.0)
    s1 = jnp.where(r1 == lane, 1.0, 0.0)
    low = jnp.where(
        lax.broadcasted_iota(jnp.int32, (ROWS, ROWS), 0) > lax.broadcasted_iota(jnp.int32, (ROWS, ROWS), 1), 1.0, 0.0
    )
    before = mm(low.astype(BF), (s0 + s1).astype(BF))
    k0 = jnp.sum(before * s0, axis=1, keepdims=True)
    k1 = jnp.sum((before + s0) * s1, axis=1, keepdims=True)
    slots = lax.broadcasted_iota(jnp.int32, (ROWS, SL), 1).astype(F32)
    c0 = jnp.where(r0.astype(F32) * CAP + k0 == slots, 1.0, 0.0)
    c1 = jnp.where(r1.astype(F32) * CAP + k1 == slots, 1.0, 0.0)
    pick[0:ROWS, :] = c0.astype(BF)
    pick[ROWS : 2 * ROWS, :] = c1.astype(BF)

    loads[0].wait()
    wide = xin[...].astype(F32)
    scale = lax.rsqrt(jnp.mean(wide * wide, axis=-1, keepdims=True) + 1e-06)
    normed = (wide * scale * gain_ref[...].astype(F32)).astype(BF)
    chosen = jnp.transpose(c0 + c1).astype(BF)
    obuf[...] = mm(chosen, normed).astype(BF)
    for g in range(SL // 16):
        rows_to_tiles(perm, obuf, 16 * g, send, 256 * g)

    pl.semaphore_wait(barrier, NE - 1 + 2)

    for q in range(NZ):
        far = ((z + DZ[q]) % NZ) * NYC

        def ship(j, _, q=q, far=far):
            to = far + (yc + j) % NYC
            pltpu.make_async_remote_copy(
                src_ref=send.at[pl.ds(pl.multiple_of(to * CH, CH), CH), :],
                dst_ref=recv.at[t, pl.ds(pl.multiple_of(q * QR + yc * CH, CH), CH), :],
                send_sem=as_sem,
                recv_sem=a_sem.at[q],
                device_id=(to, t),
                device_id_type=MESH,
            ).start()
            return 0

        lax.fori_loop(1 if q == 0 else 0, NYC, ship, 0)
    recv[t, pl.ds(pl.multiple_of(yc * CH, CH), CH), :] = send[pl.ds(pl.multiple_of(me * CH, CH), CH), :]

    def chunk(src, q):
        return recv.at[src, pl.ds(q * QR, QR), :]

    def hop(src, q, sem, x):
        return pltpu.make_async_remote_copy(
            src_ref=chunk(src, q), dst_ref=chunk(src, q), send_sem=xs_sem, recv_sem=sem.at[q],
            device_id=(me, x), device_id_type=MESH,
        )

    def arrive(q):
        n = QR - CH if q == 0 else QR
        pltpu.make_async_remote_copy(
            src_ref=send.at[pl.ds(0, n), :], dst_ref=recv.at[t, pl.ds(q * QR, n), :],
            send_sem=as_sem, recv_sem=a_sem.at[q], device_id=(me, right), device_id_type=MESH,
        ).wait_recv()

    def spread(q):
        arrive(q)
        hop(t, q, gl_sem, right).start()
        hop(t, q, gr_sem, left).start()

    def relay(q):
        if q % 2 == 0:
            hop(left, q, gl_sem, right).wait_recv()
            hop(left, q, g2_sem, right).start()
        else:
            hop(right, q, gr_sem, left).wait_recv()
            hop(right, q, g2_sem, left).start()

    def gathered(q):
        if q % 2 == 0:
            hop(right, q, gr_sem, left).wait_recv()
        else:
            hop(left, q, gl_sem, right).wait_recv()
        hop(opp, q, g2_sem, right).wait_recv()

    def rsend(src, dst, sem, p, x):
        return pltpu.make_async_remote_copy(
            src_ref=src, dst_ref=dst.at[p], send_sem=rr_sem, recv_sem=sem.at[p], device_id=(me, x), device_id_type=MESH
        )

    def ways(p):
        return (right, left) if p % 2 == 0 else (left, right)

    def experts(p):
        gathered(2 * p)
        gathered(2 * p + 1)
        if p == 0:
            for c in loads[1:]:
                c.wait()
        for tt in range(NT):
            for g in range(PT // 16):
                at = p * 2 * QR + g * 256
                y = mm(perm, recv[tt, at : at + 256, :]).astype(BF)
                row = tt * PT + 16 * g
                for i in range(TR):
                    xb[row : row + 16, 128 * i : 128 * i + 128] = y[16 * i : 16 * i + 16, :]
        x = xb[...]
        gate = mm(x, wg[...])
        up = mm(x, wu[...])
        hidden = (gate / (1.0 + jnp.exp(-gate)) * up).astype(BF)
        for tt in range(NT):
            part[p, tt] = mm(hidden[tt * PT : (tt + 1) * PT, :], wd[...]).astype(BF)
        fwd, bwd = ways(p)
        rsend(part.at[p, opp], rs1, r1_sem, p, fwd).start()
        rsend(part.at[p, bwd], rss, rss_sem, p, bwd).start()

    def middle(p):
        fwd, bwd = ways(p)
        rsend(part.at[p, opp], rs1, r1_sem, p, fwd).wait_recv()
        sumb[p] = (rs1[p].astype(F32) + part[p, fwd].astype(F32)).astype(BF)
        rsend(sumb.at[p], rsd, rsd_sem, p, fwd).start()

    def finish(p):
        fwd, bwd = ways(p)
        rsend(part.at[p, bwd], rss, rss_sem, p, bwd).wait_recv()
        rsend(sumb.at[p], rsd, rsd_sem, p, fwd).wait_recv()
        tot[...] = (part[p, t].astype(F32) + rss[p].astype(F32) + rsd[p].astype(F32)).astype(BF)
        for g in range(PT // 16):
            rows_to_tiles(perm, tot, 16 * g, ret, p * 2 * QR + 256 * g)
        for q in (2 * p, 2 * p + 1):
            far = ((z + NZ - DZ[q]) % NZ) * NYC

            def home(j, _, q=q, far=far):
                to = (yc + j) % NYC
                pltpu.make_async_remote_copy(
                    src_ref=ret.at[pl.ds(pl.multiple_of(q * QR + to * CH, CH), CH), :],
                    dst_ref=back.at[pl.ds(pl.multiple_of(me * CH, CH), CH), :],
                    send_sem=bs_sem,
                    recv_sem=b_sem,
                    device_id=(far + to, t),
                    device_id_type=MESH,
                ).start()
                return 0

            lax.fori_loop(1 if q == 0 else 0, NYC, home, 0)
        if p == 0:
            back[pl.ds(pl.multiple_of(me * CH, CH), CH), :] = ret[pl.ds(pl.multiple_of(yc * CH, CH), CH), :]

    for step in (
        (spread, 0), (spread, 1), (relay, 0), (spread, 2), (relay, 1), (spread, 3), (relay, 2), (experts, 0),
        (spread, 4), (relay, 3), (spread, 5), (relay, 4), (experts, 1), (spread, 6), (relay, 5), (spread, 7),
        (relay, 6), (relay, 7), (middle, 0), (experts, 2), (middle, 1), (finish, 0), (experts, 3), (middle, 2),
        (finish, 1), (middle, 3), (finish, 2), (finish, 3),
    ):
        step[0](step[1])

    n = ALL - CH
    last = pltpu.make_async_remote_copy(
        src_ref=ret.at[pl.ds(0, n), :], dst_ref=back.at[pl.ds(0, n), :], send_sem=bs_sem, recv_sem=b_sem,
        device_id=(me, right), device_id_type=MESH,
    )
    last.wait_recv()
    for g in range(SL // 16):
        y = mm(perm, back[256 * g : 256 * g + 256, :]).astype(BF)
        for i in range(TR):
            resb[16 * g : 16 * g + 16, 128 * i : 128 * i + 128] = y[16 * i : 16 * i + 16, :]
    picked = mm(pick[...], resb[...])
    w = rw_ref[own, :]
    out_ref[...] = (w[:, 0:1] * picked[0:ROWS, :] + w[:, 1:2] * picked[ROWS : 2 * ROWS, :]).astype(BF)

    last.wait_send()
    pltpu.make_async_remote_copy(
        src_ref=send.at[pl.ds(0, n), :], dst_ref=recv.at[t, pl.ds(0, n), :], send_sem=as_sem, recv_sem=a_sem.at[0],
        device_id=(me, right), device_id_type=MESH,
    ).wait_send()
    pltpu.make_async_remote_copy(
        src_ref=recv.at[pl.ds(0, 3)], dst_ref=recv.at[pl.ds(0, 3)], send_sem=xs_sem, recv_sem=gl_sem.at[0],
        device_id=(me, right), device_id_type=MESH,
    ).wait_send()
    pltpu.make_async_remote_copy(
        src_ref=part.at[:, pl.ds(0, 3)], dst_ref=part.at[:, pl.ds(0, 3)], send_sem=rr_sem, recv_sem=r1_sem.at[0],
        device_id=(me, right), device_id_type=MESH,
    ).wait_send()


def expert_half(routed_input, norm_gain, routes, route_weight, expert_gate, expert_up, expert_down):
    vmem = pl.BlockSpec(memory_space=pltpu.VMEM)
    hbm = pl.BlockSpec(memory_space=pl.ANY)
    dma = pltpu.SemaphoreType.DMA
    return pl.pallas_call(
        moe_kernel,
        out_shape=jax.ShapeDtypeStruct((ROWS, D), BF),
        in_specs=[hbm, vmem, vmem, vmem, hbm, hbm, hbm],
        out_specs=vmem,
        scratch_shapes=[
            pltpu.VMEM((ROWS, D), BF),
            pltpu.VMEM((SL, D), BF),
            pltpu.VMEM((2 * ROWS, SL), BF),
            pltpu.VMEM((ALL, 128), BF),
            pltpu.VMEM((NT, ALL, 128), BF),
            pltpu.VMEM((D, HID), BF),
            pltpu.VMEM((D, HID), BF),
            pltpu.VMEM((HID, D), BF),
            pltpu.VMEM((NT * PT, D), BF),
            pltpu.VMEM((NP, NT, PT, D), BF),
            pltpu.VMEM((NP, PT, D), BF),
            pltpu.VMEM((NP, PT, D), BF),
            pltpu.VMEM((NP, PT, D), BF),
            pltpu.VMEM((NP, PT, D), BF),
            pltpu.VMEM((PT, D), BF),
            pltpu.VMEM((ALL, 128), BF),
            pltpu.VMEM((ALL, 128), BF),
            pltpu.VMEM((SL, D), BF),
            dma((4,)),
            dma,
            dma((NZ,)),
            dma,
            dma((NZ,)),
            dma((NZ,)),
            dma((NZ,)),
            dma,
            dma((NP,)),
            dma((NP,)),
            dma((NP,)),
            dma,
            dma,
        ],
        compiler_params=pltpu.CompilerParams(
            collective_id=0, has_side_effects=True, vmem_limit_bytes=40 * 1024 * 1024
        ),
        cost_estimate=pl.CostEstimate(flops=60_000_000_000, bytes_accessed=8_000_000, transcendentals=0),
        name="experts",
    )(
        routed_input, routes, route_weight, norm_gain.reshape(1, D),
        expert_gate[0], expert_up[0], expert_down[0],
    )
def side_by_side(arrays, axis, dim, along):
    both = jnp.concatenate(arrays, axis=along)
    out, at, gathered = (lax.all_gather(both, axis, axis=dim, tiled=True), 0, [])
    for a in arrays:
        gathered.append(lax.slice_in_dim(out, at, at + a.shape[along], axis=along))
        at += a.shape[along]
    return tuple(gathered)


def mixer_half(queries, key_cache, value_cache, cum_gate, out_weight):
    seq_rows = queries.shape[0]
    local_heads = key_cache.shape[0]
    head_size = key_cache.shape[1]
    group = queries.shape[1] // (local_heads * head_size)
    own_start = lax.axis_index("ep") * seq_rows
    query_heads = queries.reshape(seq_rows, local_heads, group, head_size)
    query_pos = own_start + jnp.arange(seq_rows, dtype=jnp.int32)
    gate_query = lax.dynamic_slice_in_dim(cum_gate, own_start, seq_rows, 1)
    gate_rows = jnp.transpose(gate_query)[:, :, None, None]
    scale = head_size ** (-0.5)
    best_start = jnp.full((seq_rows, local_heads, group), -jnp.inf, jnp.float32)
    total_start = jnp.zeros((seq_rows, local_heads, group), jnp.float32)
    summed_start = jnp.zeros((seq_rows, local_heads * group * head_size), jnp.float32)
    pieces = side_by_side((key_cache, value_cache), "ep", 2, 0)

    def update(state):
        best, total, summed = state
        key_piece, value_piece = pieces
        width = key_piece.shape[2]
        scores = (
            jnp.einsum("thgd,hds->thgs", query_heads, key_piece, preferred_element_type=jnp.float32)
            * scale
        )
        scores = scores + gate_rows - cum_gate[None, :, None, :]
        key_pos = jnp.arange(width, dtype=jnp.int32)
        allowed = key_pos[None, :] <= query_pos[:, None]
        scores = jnp.where(allowed[:, None, None, :], scores, -jnp.inf)
        new_best = jnp.max(scores, axis=-1)
        factor = jnp.exp(best - new_best)
        weights = jnp.exp(scores - new_best[..., None])
        new_total = total * factor + jnp.sum(weights, axis=-1)
        product = jnp.einsum(
            "thgs,hds->thgd",
            weights.astype(jnp.bfloat16),
            value_piece,
            preferred_element_type=jnp.float32,
        )
        new_summed = summed.reshape(product.shape) * factor[..., None] + product
        return (new_best, new_total, new_summed.reshape(seq_rows, local_heads * group * head_size))

    best, total, summed = lax.cond(
        jnp.int32(0) <= own_start,
        update,
        lambda state: state,
        (best_start, total_start, summed_start),
    )
    attended = summed.reshape(seq_rows, local_heads, group, head_size) / total[..., None]
    attended = attended.astype(jnp.bfloat16).reshape(seq_rows, local_heads * group * head_size)
    by_position = lax.all_to_all(attended, "tp", split_axis=0, concat_axis=1, tiled=True)
    return jnp.dot(by_position, out_weight, preferred_element_type=jnp.float32).astype(jnp.bfloat16)


def body(
    queries,
    key_cache,
    value_cache,
    cum_gate,
    out_weight,
    routed_input,
    norm_gain,
    routes,
    route_weight,
    expert_gate,
    expert_up,
    expert_down,
):
    mixed_out = mixer_half(queries, key_cache, value_cache, cum_gate, out_weight)
    expert_out = expert_half(
        routed_input, norm_gain, routes, route_weight, expert_gate, expert_up, expert_down
    )
    return (mixed_out, expert_out)


def solution(mesh):
    return jax.shard_map(
        body,
        mesh=mesh,
        in_specs=(
            P("ep", "tp"),
            P("tp", None, "ep"),
            P("tp", None, "ep"),
            P("tp", None),
            P(),
            P("ep", None),
            P(),
            P("ep", None),
            P("ep", None),
            P("ep", None, "tp"),
            P("ep", None, "tp"),
            P("ep", "tp", None),
        ),
        out_specs=(P(("ep", "tp"), None), P(("ep", "tp"), None)),
        check_vma=False,
    )
```

time: 211 us -> 205 us (0.972)
  Pallas kernels: 0 us -> 89.7 us
  blocking collectives: 41.1 us -> 0 us
  starting transfers between devices: 23 us -> 4.01 us
  matrix products: 22.4 us -> 6.4 us
  waiting for transfers between devices: 90 us -> 76.5 us
  other arithmetic: 7.98 us -> 3.3 us
    pallas_call x0 -> x1, Pallas kernels: none -> 89.7 us  [expert_half(): pl.pallas_call(moe_kernel, out_shape=jax.ShapeDtypeStruct((ROWS, D), BF),...]
    all_to_all x3 -> x0, waiting for transfers between devices: 69 us -> none  [the longest x1 35.8 us: copy_for_each(): lax.all_to_all(jnp.broadcast_to(x[None], (count, *x.shape)), axis, 0, 0,...]
    all_gather x1, waiting for transfers between devices: 21 us -> 76.4 us  [side_by_side(): lax.all_gather(both, axis, axis=dim, tiled=True)]
    all_to_all x1 -> x0, blocking collectives: 41.1 us -> none  [expert_half(): lax.all_to_all(outgoing.reshape(1, ep_size, per_device, width), 'ep', spl...]
    all_to_all x3 -> x0, starting transfers between devices: 19.5 us -> none  [the longest x1 10.1 us: expert_half(): lax.all_to_all(summed.astype(jnp.bfloat16), 'ep', split_axis=1, concat_ax...]
    dot_general x4 -> x0, matrix products: 16 us -> none  [the longest x1 7.72 us: expert_half(): jnp.einsum('abecf,efd->abecd', hidden, expert_down, preferred_element_typ...]
    unnamed x14 -> x13, local copies, waits for them, and re-layouts: 0.04 us -> 7.23 us
    reduce_sum x4 -> x0, other arithmetic: 3.82 us -> none  [the longest x1 2.46 us: sum_at_owner(): return jnp.sum(parts.astype(jnp.float32), axis=0)]
  transfers between devices with their start and end apart: 5 -> 2, of which waited for: 4 -> 1; matrix products, arithmetic and copies ran while one was open for 12% -> 1% of each run, Pallas kernels for 0% -> 44%
where the time goes in v1:
time: 205 us
  Pallas kernels  89.7 us (44%)
  waiting for transfers between devices  76.5 us (37%)
  between operations  14.1 us (7%)
  local copies, waits for them, and re-layouts  10.7 us (5%)
  matrix products  6.4 us (3%)
  starting transfers between devices  4.01 us (2%)
  other arithmetic  3.3 us (2%)
    pallas_call x1, Pallas kernels, expert_half(): pl.pallas_call(moe_kernel, out_shape=jax.ShapeDtypeStruct((ROWS, D), BF),...  89.7 us
    all_gather x1, waiting for transfers between devices, side_by_side(): lax.all_gather(both, axis, axis=dim, tiled=True)  76.4 us
    unnamed x13, local copies, waits for them, and re-layouts  7.23 us
  transfers between devices with their start and end apart: 2, of which 1 were waited for; matrix products, arithmetic and copies ran while one was open for 1% of the time, Pallas kernels for 44%

profile of v1, /device:TPU:1, one launch (start us, length us, event | category | flops | bytes accessed | tf_op | source)
XLA Modules:
  0.0 204.7 jit_solution(13759353649421636241)
XLA Ops:
  7.2 0.0 copy-start
  7.2 0.0 all-gather.2.cloned.1.call-start
  7.2 1.5 pad_maximum_fusion
  8.7 0.0 all-gather.2.cloned.1.call-update
  8.7 0.8 copy.31.routes_ref
  9.6 0.8 copy.32.rw_ref
  10.4 0.7 reshape.141.gain_ref
  11.1 76.4 %all-gather.2.cloned.1.call-done = bf16[2,64,8192]{2,1,0:T(8,128)(2,1)} async-done(((bf16[2,64,128]{2,1,0:T(8,128)(2,1)}), bf16[2,64,8192]{2,1,0:T(8,128)(2,1)}) %all-gather.2.cloned.1.call-update) | async-done | bytes 2097168 | tf_op jit(solution)/shard_map/all_gather | solution.py:320
  87.5 9.2 %conditional.1 = (f32[128,1,2]{0,2,1:T(2,128)S(1)}, f32[128,128]{0,1:T(8,128)S(1)}) conditional(s32[]{:T(128)} %convert_element_type.16, () %tuple.19, (s32[]{:T(128)}, s32[128]{0:T(128)S(1)}, bf16[2,64,8192]{2,1,0:T(8,128)(2,1)}, bf16[128,128]{1,0:T(8,128)(2,1)}, f32[1,8192]{1,0:T(1,128)}) %tuple.20), branch_computations={%region_0.0_spmd, %region_1.4_spmd} | conditional | flops 556810624 | bytes 37957720 | solution.py:368
  87.5 0.8 dynamic-slice_bitcast_fusion
  88.3 0.7 iota_compare_fusion
  89.0 0.9 copy.28
  89.8 3.9 %fusion.24 = (f32[128,2]{0,1:T(2,128)S(1)}, f32[128,1,2,8192]{0,3,2,1:T(8,128)S(1)}) fusion(f32[8192]{0:T(1024)} %bitcast.71, f32[128]{0:T(128)S(1)} %dynamic-slice_bitcast_fusion, bf16[128,2,64]{0,2,1:T(8,128)(2,1)S(1)} %bitcast.69, bf16[2,64,8192]{2,1,0:T(8,128)(2,1)} %get-tuple-element.52, pred[128,8192]{0,1:T(8,128)(4,1)S(1)} %iota_compare_fusion), kind=kOutput, calls=%fused_computation.29 | convolution fusion | flops 278920960 | bytes 10552832 | tf_op jit(solution)/shard_map/cond/branch_1_fun/thgd,hds->thgs/dot_general | solution.py:348
  93.7 0.0 copy-start.5
  93.7 1.1 fusion.6
  94.8 0.5 copy-done.5
  95.3 1.4 fusion.14
  96.7 0.7 copy.29
  97.5 4.0 %all-to-all-start = ((bf16[4,32,128]{2,1,0:T(8,128)(2,1)}), bf16[4,32,128]{2,1,0:T(8,128)(2,1)S(1)}, u32[]{:S(2)}, u32[]{:S(2)}) async-start(bf16[4,32,128]{2,1,0:T(8,128)(2,1)} %bitcast.17), calls=%async_computation | async-start | bytes 65536 | tf_op jit(solution)/shard_map/all_to_all | solution.py:376
  101.4 0.0 copy-start.1
  101.4 1.2 copy-done.1
  102.6 0.0 copy-start.2
  102.7 1.2 copy-done.2
  103.9 0.0 copy-start.3
  103.9 1.2 copy-done.3
  105.1 0.0 copy-start.4
  105.1 1.2 copy-done.4
  106.3 89.7 %experts.1 = bf16[64,2048]{1,0:T(8,128)(2,1)S(1)} custom-call(bf16[256,2048]{1,0:T(8,128)(2,1)S(1)} %copy-done.1, s32[256,2]{1,0:T(8,128)S(1)} %copy.31.routes_ref, f32[256,2]{1,0:T(8,128)S(1)} %copy.32.rw_ref, bf16[1,2048]{1,0:T(2,128)(2,1)S(1)} %reshape.141.gain_ref, bf16[2048,256]{1,0:T(8,128)(2,1)S(1)} %bitcast.65, bf16[2048,256]{1,0:T(8,128)(2,1)S(1)} %bitcast.66, ...), custom_call_target="tpu_custom_call" | custom-call | flops 60000002048 | bytes 8000000 | tf_op jit(solution)/shard_map/experts/pallas_call | solution.py:271
  196.0 0.0 all-to-all-done
  196.0 0.0 copy-done
  196.0 1.1 convolution_convert_fusion
  197.2 0.7 copy.44
  (4 shorter events, 0.0 us)
Async XLA Ops:
  7.2 188.9 %copy-start = (bf16[512,2048]{1,0:T(8,128)(2,1)S(1)}, bf16[512,2048]{1,0:T(8,128)(2,1)}, u32[]{:S(2)}) copy-start(bf16[512,2048]{1,0:T(8,128)(2,1)} %param.18) | copy-start | bytes 6291460
  7.2 80.4 %all-gather.2.cloned.1.call-start = ((), (), s32[]{:S(2)}) async-start(), calls=%async_computation.1 | async-start | bytes 2129920 | tf_op jit(solution)/shard_map/all_gather | solution.py:320
  93.7 1.6 copy-start.5
  97.5 98.6 %all-to-all-start = ((bf16[4,32,128]{2,1,0:T(8,128)(2,1)}), bf16[4,32,128]{2,1,0:T(8,128)(2,1)S(1)}, u32[]{:S(2)}, u32[]{:S(2)}) async-start(bf16[4,32,128]{2,1,0:T(8,128)(2,1)} %bitcast.17), calls=%async_computation | async-start | bytes 65536 | tf_op jit(solution)/shard_map/all_to_all | solution.py:376
  101.4 1.2 copy-start.1
  102.6 1.2 copy-start.2
  103.9 1.2 copy-start.3
  105.1 1.2 copy-start.4
Sparse Core Ops, SparseCore 0:
  11.2 76.2 all-gather.1

commit v2 on v1

--- a/solution.py
+++ b/solution.py
@@ -1,5 +1,3 @@
-import functools
-
 import jax
 import jax.numpy as jnp
 from jax import lax
@@ -26,6 +24,10 @@
 NP = NZ // 2
 PT = 2 * NYC * CAP
 HID = 256
+NY = 4
+HEAD = 64
+SEQ = 128
+MIX = SEQ // NT
 DZ = (0, 1, 7, 2, 6, 3, 5, 4)
 
 
@@ -45,16 +47,19 @@
     dst[at : at + 256, :] = mm(perm, z).astype(BF)
 
 
-def moe_kernel(
-    x_hbm, routes_ref, rw_ref, gain_ref, wg_hbm, wu_hbm, wd_hbm,
-    out_ref,
-    xin, obuf, pick, send, recv, wg, wu, wd, xb, part, rs1, rss, rsd, sumb, tot, ret, back, resb,
+def layer_kernel(
+    x_hbm, routes_ref, rw_ref, gain_ref, wg_hbm, wu_hbm, wd_hbm, q_ref, key_hbm, value_hbm, gate_ref, wo_hbm,
+    out_ref, mix_ref,
+    xin, obuf, pick, send, recv, wg, wu, wd, xb, part, rs1, rss, rsd, sumb, tot, ret, back, resb, kv, wo, att, att_all,
     ld_sem, as_sem, a_sem, xs_sem, gl_sem, gr_sem, g2_sem, rr_sem, r1_sem, rss_sem, rsd_sem, bs_sem, b_sem,
+    ks_sem, ku_sem, kd_sem, yu_sem, yd_sem, pc_sem, ts_sem, t_sem,
 ):
     t = lax.axis_index("tp")
     me = lax.axis_index("ep")
     z = me // NYC
     yc = me % NYC
+    y = yc // 2
+    c = yc % 2
     right = (t + 1) % NT
     left = (t + 3) % NT
     opp = (t + 2) % NT
@@ -64,9 +69,12 @@
         pltpu.make_async_copy(wg_hbm, wg, ld_sem.at[1]),
         pltpu.make_async_copy(wu_hbm, wu, ld_sem.at[2]),
         pltpu.make_async_copy(wd_hbm, wd, ld_sem.at[3]),
+        pltpu.make_async_copy(wo_hbm, wo, ld_sem.at[4]),
+        pltpu.make_async_copy(key_hbm, kv.at[z, y, c, pl.ds(0, HEAD), :], ld_sem.at[5]),
+        pltpu.make_async_copy(value_hbm, kv.at[z, y, c, pl.ds(HEAD, HEAD), :], ld_sem.at[6]),
     ]
-    for c in loads:
-        c.start()
+    for load in loads:
+        load.start()
 
     barrier = pltpu.get_barrier_semaphore()
 
@@ -75,10 +83,139 @@
         return 0
 
     lax.fori_loop(1, NE, greet, 0)
-    for x in (right, left):
+    for x in (right, left, opp):
         pl.semaphore_signal(barrier, inc=1, device_id=(me, x), device_id_type=MESH)
 
     perm = permutation()
+
+    def kv_send(block, sem, to, way=0):
+        return pltpu.make_async_remote_copy(
+            src_ref=block, dst_ref=block, send_sem=ks_sem.at[way], recv_sem=sem, device_id=(to, t), device_id_type=MESH
+        )
+
+    def at_z(dz):
+        return ((z + dz + NZ) % NZ) * NYC + yc
+
+    def at_y(dy):
+        return z * NYC + ((y + dy + NY) % NY) * 2 + c
+
+    def kv_up(d):
+        block = kv.at[(z + NZ - d) % NZ, y, c]
+        if d > 0:
+            kv_send(block, ku_sem.at[d - 1], at_z(1)).wait_recv()
+        if d < NZ // 2:
+            kv_send(block, ku_sem.at[d], at_z(1)).start()
+
+    def kv_down(d):
+        block = kv.at[(z + d) % NZ, y, c]
+        if d > 0:
+            kv_send(block, kd_sem.at[d - 1], at_z(-1)).wait_recv()
+        if d < NZ // 2 - 1:
+            kv_send(block, kd_sem.at[d], at_z(-1)).start()
+
+    def column(dy):
+        return kv.at[:, (y + dy + NY) % NY, c]
+
+    def half(dy, up):
+        return kv.at[pl.ds(0 if up else NZ // 2, NZ // 2), (y + dy + NY) % NY, c]
+
+    partner = z * NYC + y * 2 + 1 - c
+
+    def kv_rows(step):
+        if step == 0:
+            kv_send(column(0), yu_sem.at[0], at_y(1), 1).start()
+            kv_send(column(0), yd_sem.at[0], at_y(-1), 1).start()
+            kv_send(column(0), pc_sem.at[0], partner, 2).start()
+        elif step == 1:
+            kv_send(column(-1), yu_sem.at[0], at_y(1), 1).wait_recv()
+            kv_send(half(-1, True), yu_sem.at[1], at_y(1), 1).start()
+            kv_send(column(-1), pc_sem.at[1], partner, 2).start()
+            kv_send(column(1), yd_sem.at[0], at_y(-1), 1).wait_recv()
+            kv_send(half(1, False), yd_sem.at[1], at_y(-1), 1).start()
+            kv_send(column(1), pc_sem.at[2], partner, 2).start()
+        elif step == 2:
+            kv_send(half(2, True), yu_sem.at[1], at_y(1), 1).wait_recv()
+            kv_send(half(2, False), yd_sem.at[1], at_y(-1), 1).wait_recv()
+            kv_send(column(2), pc_sem.at[3], partner, 2).start()
+        else:
+            for k, dy in enumerate((0, -1, 1, 2)):
+                other = kv.at[:, (y + dy + NY) % NY, 1 - c]
+                kv_send(other, pc_sem.at[k], partner, 2).wait_recv()
+
+    def kv_step(d):
+        kv_up(d)
+        if d < NZ // 2:
+            kv_down(d)
+
+    def attend(_):
+        lane = lax.broadcasted_iota(jnp.int32, (SEQ, 2 * HEAD), 1)
+        q = q_ref[...].astype(F32) * (HEAD**-0.5)
+        q = jnp.concatenate([jnp.where(lane < HEAD, q, 0.0), jnp.where(lane < HEAD, 0.0, q)], axis=0).astype(BF)
+        own_gate = gate_ref[0:1, pl.ds(pl.multiple_of(me * SEQ, SEQ), SEQ)]
+        column_gate = jnp.transpose(jnp.broadcast_to(own_gate, (SEQ, SEQ)))[:, 0:1]
+        gq = jnp.concatenate([column_gate, column_gate], axis=0)
+        wide = NYC * SEQ
+
+        def scored(plane):
+            keys = []
+            for k in range(NYC):
+                block = kv[plane, k // 2, k % 2, 0:HEAD, :]
+                keys.append(jnp.concatenate([block, block], axis=0))
+            gk = gate_ref[0:1, pl.ds(pl.multiple_of(plane * wide, wide), wide)]
+            return mm(q, jnp.concatenate(keys, axis=1)) + (gq - gk)
+
+        def folded(w):
+            total = w[:, 0:SEQ]
+            for k in range(1, NYC):
+                total = total + w[:, k * SEQ : (k + 1) * SEQ]
+            return total
+
+        def mixed(plane, w):
+            values = []
+            for k in range(NYC):
+                block = kv[plane, k // 2, k % 2, HEAD : 2 * HEAD, :]
+                values.append(jnp.concatenate([block, block], axis=0))
+            return lax.dot_general(
+                w.astype(BF), jnp.concatenate(values, axis=1), (((1,), (1,)), ((), ())), preferred_element_type=F32
+            )
+
+        rows = lax.broadcasted_iota(jnp.int32, (2 * SEQ, wide), 0) & (SEQ - 1)
+        cols = lax.broadcasted_iota(jnp.int32, (2 * SEQ, wide), 1)
+        s = jnp.where(cols <= rows + yc * SEQ, scored(z), -jnp.inf)
+        best = jnp.max(s, axis=1, keepdims=True)
+        w = jnp.exp(s - best)
+
+        def plane_step(plane, state):
+            best, total, summed = state
+            s = scored(plane)
+            new = jnp.maximum(best, jnp.max(s, axis=1, keepdims=True))
+            factor = jnp.exp(best - new)
+            w = jnp.exp(s - new)
+            return new, total * factor + folded(w), summed * factor + mixed(plane, w)
+
+        best, total, summed = lax.fori_loop(0, z, plane_step, (best, folded(w), mixed(z, w)))
+        result = summed / jnp.sum(total, axis=1, keepdims=True)
+        result = jnp.where(lane < HEAD, result[0:SEQ, :], result[SEQ : 2 * SEQ, :])
+        att[...] = result.astype(BF)
+        for k, x in enumerate((right, left, opp)):
+            att_send(k, x).start()
+        att_all[t] = att[pl.ds(pl.multiple_of(t * MIX, MIX), MIX), :]
+
+    def att_send(k, x):
+        return pltpu.make_async_remote_copy(
+            src_ref=att.at[pl.ds(pl.multiple_of(x * MIX, MIX), MIX), :], dst_ref=att_all.at[t],
+            send_sem=ts_sem, recv_sem=t_sem.at[k], device_id=(me, x), device_id_type=MESH,
+        )
+
+    def project(_):
+        for k, x in enumerate((left, right, opp)):
+            pltpu.make_async_remote_copy(
+                src_ref=att_all.at[x], dst_ref=att_all.at[x], send_sem=ts_sem, recv_sem=t_sem.at[k],
+                device_id=(me, x), device_id_type=MESH,
+            ).wait_recv()
+        loads[4].wait()
+        joined = jnp.concatenate([att_all[k] for k in range(NT)], axis=1)
+        mix_ref[...] = mm(joined, wo[...]).astype(BF)
 
     own = pl.ds(pl.multiple_of(t * ROWS, ROWS), ROWS)
     r = routes_ref[own, :]
@@ -108,7 +245,11 @@
     for g in range(SL // 16):
         rows_to_tiles(perm, obuf, 16 * g, send, 256 * g)
 
-    pl.semaphore_wait(barrier, NE - 1 + 2)
+    loads[5].wait()
+    loads[6].wait()
+    pl.semaphore_wait(barrier, NE - 1 + 3)
+    kv_up(0)
+    kv_down(0)
 
     for q in range(NZ):
         far = ((z + DZ[q]) % NZ) * NYC
@@ -176,8 +317,8 @@
         gathered(2 * p)
         gathered(2 * p + 1)
         if p == 0:
-            for c in loads[1:]:
-                c.wait()
+            for load in loads[1:4]:
+                load.wait()
         for tt in range(NT):
             for g in range(PT // 16):
                 at = p * 2 * QR + g * 256
@@ -228,10 +369,12 @@
             back[pl.ds(pl.multiple_of(me * CH, CH), CH), :] = ret[pl.ds(pl.multiple_of(yc * CH, CH), CH), :]
 
     for step in (
-        (spread, 0), (spread, 1), (relay, 0), (spread, 2), (relay, 1), (spread, 3), (relay, 2), (experts, 0),
-        (spread, 4), (relay, 3), (spread, 5), (relay, 4), (experts, 1), (spread, 6), (relay, 5), (spread, 7),
-        (relay, 6), (relay, 7), (middle, 0), (experts, 2), (middle, 1), (finish, 0), (experts, 3), (middle, 2),
-        (finish, 1), (middle, 3), (finish, 2), (finish, 3),
+        (spread, 0), (kv_step, 1), (spread, 1), (relay, 0), (kv_step, 2), (spread, 2), (relay, 1), (kv_step, 3),
+        (spread, 3), (relay, 2), (kv_step, 4), (kv_rows, 0), (experts, 0),
+        (spread, 4), (relay, 3), (kv_rows, 1), (spread, 5), (relay, 4), (kv_rows, 2), (experts, 1), (spread, 6),
+        (relay, 5), (spread, 7), (relay, 6), (relay, 7), (middle, 0), (kv_rows, 3), (attend, 0),
+        (experts, 2), (middle, 1), (finish, 0), (experts, 3), (middle, 2),
+        (finish, 1), (project, 0), (middle, 3), (finish, 2), (finish, 3),
     ):
         step[0](step[1])
 
@@ -251,6 +394,22 @@
 
     last.wait_send()
     pltpu.make_async_remote_copy(
+        src_ref=kv.at[:, pl.ds(0, 3), 0], dst_ref=kv.at[:, pl.ds(0, 3), 0], send_sem=ks_sem.at[1], recv_sem=ku_sem.at[0],
+        device_id=(me, right), device_id_type=MESH,
+    ).wait_send()
+    pltpu.make_async_remote_copy(
+        src_ref=kv.at[:, :, 0], dst_ref=kv.at[:, :, 0], send_sem=ks_sem.at[2], recv_sem=ku_sem.at[0],
+        device_id=(me, right), device_id_type=MESH,
+    ).wait_send()
+    pltpu.make_async_remote_copy(
+        src_ref=kv.at[pl.ds(0, NZ - 1), 0, 0], dst_ref=kv.at[pl.ds(0, NZ - 1), 0, 0], send_sem=ks_sem.at[0],
+        recv_sem=ku_sem.at[0], device_id=(me, right), device_id_type=MESH,
+    ).wait_send()
+    pltpu.make_async_remote_copy(
+        src_ref=att.at[pl.ds(0, 3 * MIX), :], dst_ref=att.at[pl.ds(0, 3 * MIX), :], send_sem=ts_sem,
+        recv_sem=t_sem.at[0], device_id=(me, right), device_id_type=MESH,
+    ).wait_send()
+    pltpu.make_async_remote_copy(
         src_ref=send.at[pl.ds(0, n), :], dst_ref=recv.at[t, pl.ds(0, n), :], send_sem=as_sem, recv_sem=a_sem.at[0],
         device_id=(me, right), device_id_type=MESH,
     ).wait_send()
@@ -264,15 +423,28 @@
     ).wait_send()
 
 
-def expert_half(routed_input, norm_gain, routes, route_weight, expert_gate, expert_up, expert_down):
+def body(
+    queries,
+    key_cache,
+    value_cache,
+    cum_gate,
+    out_weight,
+    routed_input,
+    norm_gain,
+    routes,
+    route_weight,
+    expert_gate,
+    expert_up,
+    expert_down,
+):
     vmem = pl.BlockSpec(memory_space=pltpu.VMEM)
     hbm = pl.BlockSpec(memory_space=pl.ANY)
     dma = pltpu.SemaphoreType.DMA
-    return pl.pallas_call(
-        moe_kernel,
-        out_shape=jax.ShapeDtypeStruct((ROWS, D), BF),
-        in_specs=[hbm, vmem, vmem, vmem, hbm, hbm, hbm],
-        out_specs=vmem,
+    expert_out, mixed_out = pl.pallas_call(
+        layer_kernel,
+        out_shape=(jax.ShapeDtypeStruct((ROWS, D), BF), jax.ShapeDtypeStruct((MIX, D), BF)),
+        in_specs=[hbm, vmem, vmem, vmem, hbm, hbm, hbm, vmem, hbm, hbm, vmem, hbm],
+        out_specs=(vmem, vmem),
         scratch_shapes=[
             pltpu.VMEM((ROWS, D), BF),
             pltpu.VMEM((SL, D), BF),
@@ -292,7 +464,11 @@
             pltpu.VMEM((ALL, 128), BF),
             pltpu.VMEM((ALL, 128), BF),
             pltpu.VMEM((SL, D), BF),
-            dma((4,)),
+            pltpu.VMEM((NZ, NY, 2, 2 * HEAD, SEQ), BF),
+            pltpu.VMEM((NT * 2 * HEAD, D), BF),
+            pltpu.VMEM((SEQ, 2 * HEAD), BF),
+            pltpu.VMEM((NT, MIX, 2 * HEAD), BF),
+            dma((7,)),
             dma,
             dma((NZ,)),
             dma,
@@ -305,95 +481,22 @@
             dma((NP,)),
             dma,
             dma,
+            dma((3,)),
+            dma((4,)),
+            dma((3,)),
+            dma((2,)),
+            dma((2,)),
+            dma((4,)),
+            dma,
+            dma((3,)),
         ],
-        compiler_params=pltpu.CompilerParams(
-            collective_id=0, has_side_effects=True, vmem_limit_bytes=40 * 1024 * 1024
-        ),
+        compiler_params=pltpu.CompilerParams(collective_id=0, has_side_effects=True, vmem_limit_bytes=67043328),
         cost_estimate=pl.CostEstimate(flops=60_000_000_000, bytes_accessed=8_000_000, transcendentals=0),
-        name="experts",
+        name="layer",
     )(
         routed_input, routes, route_weight, norm_gain.reshape(1, D),
         expert_gate[0], expert_up[0], expert_down[0],
-    )
-def side_by_side(arrays, axis, dim, along):
-    both = jnp.concatenate(arrays, axis=along)
-    out, at, gathered = (lax.all_gather(both, axis, axis=dim, tiled=True), 0, [])
-    for a in arrays:
-        gathered.append(lax.slice_in_dim(out, at, at + a.shape[along], axis=along))
-        at += a.shape[along]
-    return tuple(gathered)
-
-
-def mixer_half(queries, key_cache, value_cache, cum_gate, out_weight):
-    seq_rows = queries.shape[0]
-    local_heads = key_cache.shape[0]
-    head_size = key_cache.shape[1]
-    group = queries.shape[1] // (local_heads * head_size)
-    own_start = lax.axis_index("ep") * seq_rows
-    query_heads = queries.reshape(seq_rows, local_heads, group, head_size)
-    query_pos = own_start + jnp.arange(seq_rows, dtype=jnp.int32)
-    gate_query = lax.dynamic_slice_in_dim(cum_gate, own_start, seq_rows, 1)
-    gate_rows = jnp.transpose(gate_query)[:, :, None, None]
-    scale = head_size ** (-0.5)
-    best_start = jnp.full((seq_rows, local_heads, group), -jnp.inf, jnp.float32)
-    total_start = jnp.zeros((seq_rows, local_heads, group), jnp.float32)
-    summed_start = jnp.zeros((seq_rows, local_heads * group * head_size), jnp.float32)
-    pieces = side_by_side((key_cache, value_cache), "ep", 2, 0)
-
-    def update(state):
-        best, total, summed = state
-        key_piece, value_piece = pieces
-        width = key_piece.shape[2]
-        scores = (
-            jnp.einsum("thgd,hds->thgs", query_heads, key_piece, preferred_element_type=jnp.float32)
-            * scale
-        )
-        scores = scores + gate_rows - cum_gate[None, :, None, :]
-        key_pos = jnp.arange(width, dtype=jnp.int32)
-        allowed = key_pos[None, :] <= query_pos[:, None]
-        scores = jnp.where(allowed[:, None, None, :], scores, -jnp.inf)
-        new_best = jnp.max(scores, axis=-1)
-        factor = jnp.exp(best - new_best)
-        weights = jnp.exp(scores - new_best[..., None])
-        new_total = total * factor + jnp.sum(weights, axis=-1)
-        product = jnp.einsum(
-            "thgs,hds->thgd",
-            weights.astype(jnp.bfloat16),
-            value_piece,
-            preferred_element_type=jnp.float32,
-        )
-        new_summed = summed.reshape(product.shape) * factor[..., None] + product
-        return (new_best, new_total, new_summed.reshape(seq_rows, local_heads * group * head_size))
-
-    best, total, summed = lax.cond(
-        jnp.int32(0) <= own_start,
-        update,
-        lambda state: state,
-        (best_start, total_start, summed_start),
-    )
-    attended = summed.reshape(seq_rows, local_heads, group, head_size) / total[..., None]
-    attended = attended.astype(jnp.bfloat16).reshape(seq_rows, local_heads * group * head_size)
-    by_position = lax.all_to_all(attended, "tp", split_axis=0, concat_axis=1, tiled=True)
-    return jnp.dot(by_position, out_weight, preferred_element_type=jnp.float32).astype(jnp.bfloat16)
-
-
-def body(
-    queries,
-    key_cache,
-    value_cache,
-    cum_gate,
-    out_weight,
-    routed_input,
-    norm_gain,
-    routes,
-    route_weight,
-    expert_gate,
-    expert_up,
-    expert_down,
-):
-    mixed_out = mixer_half(queries, key_cache, value_cache, cum_gate, out_weight)
-    expert_out = expert_half(
-        routed_input, norm_gain, routes, route_weight, expert_gate, expert_up, expert_down
+        queries, key_cache[0], value_cache[0], cum_gate, out_weight,
     )
     return (mixed_out, expert_out)
 

time: 205 us -> 109 us (0.53)
  waiting for transfers between devices: 76.5 us -> 0 us
  between operations: 14.1 us -> 0.64 us
  Pallas kernels: 89.7 us -> 100 us
  matrix products: 6.4 us -> 0 us
  starting transfers between devices: 4.01 us -> 0 us
  other arithmetic: 3.3 us -> 0 us
  local copies, waits for them, and re-layouts: 10.7 us -> 7.47 us
    all_gather x1 -> x0, waiting for transfers between devices: 76.4 us -> none  [side_by_side(): lax.all_gather(both, axis, axis=dim, tiled=True)]
    pallas_call x1, Pallas kernels: 89.7 us -> 100 us  [body(): pl.pallas_call(layer_kernel, out_shape=(jax.ShapeDtypeStruct((ROWS, D), B...]
    dot_general x3 -> x0, matrix products: 6.4 us -> none  [the longest x1 3.86 us: update(): jnp.einsum('thgd,hds->thgs', query_heads, key_piece, preferred_element_ty...]
    all_to_all x1 -> x0, starting transfers between devices: 3.97 us -> none  [mixer_half(): lax.all_to_all(attended, 'tp', split_axis=0, concat_axis=1, tiled=True)]
    unnamed x13 -> x4, local copies, waits for them, and re-layouts: 7.23 us -> 6.19 us
  transfers between devices with their start and end apart: 2 -> 0, of which waited for: 1 -> 0; matrix products, arithmetic and copies ran while one was open for 1% -> 0% of each run, Pallas kernels for 44% -> 0%
where the time goes in v2:
time: 109 us
  Pallas kernels  100 us (92%)
  local copies, waits for them, and re-layouts  7.47 us (7%)
    pallas_call x1, Pallas kernels, body(): pl.pallas_call(layer_kernel, out_shape=(jax.ShapeDtypeStruct((ROWS, D), B...  100 us
    unnamed x4, local copies, waits for them, and re-layouts  6.19 us

profile of v2, /device:TPU:1, one launch (start us, length us, event | category | flops | bytes accessed | tf_op | source)
XLA Modules:
  0.0 108.6 jit_solution(9183702436292520336)
XLA Ops:
  0.6 1.3 %reshape.7.gain_ref = bf16[1,2048]{1,0:T(2,128)(2,1)} reshape(bf16[2048]{0:T(1024)(128)(2,1)} %param.18) | data formatting | bytes 8192 | tf_op jit(solution)/shard_map/reshape | solution.py:497
  1.9 1.5 %copy.14.routes_ref = s32[256,2]{1,0:T(8,128)} copy(s32[256,2]{0,1:T(2,128)} %param.19) | data formatting | bytes 4096 | tf_op args[7]
  3.4 1.5 %copy.15.rw_ref = f32[256,2]{1,0:T(8,128)} copy(f32[256,2]{0,1:T(2,128)} %param.20) | data formatting | bytes 4096 | tf_op args[8]
  4.9 100.5 %layer.1 = (bf16[64,2048]{1,0:T(8,128)(2,1)}, bf16[32,2048]{1,0:T(8,128)(2,1)}) custom-call(bf16[256,2048]{1,0:T(8,128)(2,1)} %x_hbm.1, s32[256,2]{1,0:T(8,128)} %copy.14.routes_ref, f32[256,2]{1,0:T(8,128)} %copy.15.rw_ref, bf16[1,2048]{1,0:T(2,128)(2,1)} %reshape.7.gain_ref, bf16[2048,256]{1,0:T(8,128)(2,1)} %bitcast.5, bf16[2048,256]{1,0:T(8,128)(2,1)} %bitcast.6, ...), custom_call_target="tpu_custom_call" | custom-call | flops 60000002048 | bytes 8000000 | tf_op jit(solution)/shard_map/layer/pallas_call | solution.py:443
  105.4 1.6 %copy.18 = bf16[32,2048]{1,0:T(8,128)(2,1)} copy(bf16[32,2048]{1,0:T(8,128)(2,1)} %get-tuple-element.8) | data formatting | bytes 262144
  106.9 1.7 %copy.19 = bf16[64,2048]{1,0:T(8,128)(2,1)} copy(bf16[64,2048]{1,0:T(8,128)(2,1)} %get-tuple-element.9) | data formatting | bytes 524288

commit v3 on v2

--- a/solution.py
+++ b/solution.py
@@ -28,7 +28,16 @@
 HEAD = 64
 SEQ = 128
 MIX = SEQ // NT
-DZ = (0, 1, 7, 2, 6, 3, 5, 4)
+DZ = (0, 7, 2, 1, 3, 5, 6, 4)
+ORDER = (
+    ("spread", 0), ("spread", 1), ("relay", 0), ("spread", 2), ("spread", 3), ("spread", 5),
+    ("relay", 1), ("spread", 6), ("spread", 4), ("relay", 2), ("kv", 0), ("relay", 5),
+    ("relay", 4), ("spread", 7), ("relay", 3), ("kv", 1), ("relay", 6), ("kv", 2),
+    ("relay", 7), ("experts", 2), ("kv", 3), ("experts", 3), ("kv", 4), ("rows", 0),
+    ("middle", 2), ("experts", 1), ("middle", 3), ("finish", 2), ("middle", 1), ("rows", 1),
+    ("experts", 0), ("finish", 3), ("rows", 2), ("middle", 0), ("rows", 3), ("finish", 1),
+    ("attend", 0), ("finish", 0), ("project", 0),
+)
 
 
 def permutation():
@@ -48,9 +57,9 @@
 
 
 def layer_kernel(
-    x_hbm, routes_ref, rw_ref, gain_ref, wg_hbm, wu_hbm, wd_hbm, q_ref, key_hbm, value_hbm, gate_ref, wo_hbm,
+    x_ref, routes_ref, rw_ref, gain_ref, wg_hbm, wu_hbm, wd_hbm, q_ref, key_hbm, value_hbm, gate_ref, wo_hbm,
     out_ref, mix_ref,
-    xin, obuf, pick, send, recv, wg, wu, wd, xb, part, rs1, rss, rsd, sumb, tot, ret, back, resb, kv, wo, att, att_all,
+    xin, obuf, pick, wcol, send, recv, wg, wu, wd, xb, part, rs1, rss, rsd, sumb, tot, ret, back, resb, kv, wo, att, att_all,
     ld_sem, as_sem, a_sem, xs_sem, gl_sem, gr_sem, g2_sem, rr_sem, r1_sem, rss_sem, rsd_sem, bs_sem, b_sem,
     ks_sem, ku_sem, kd_sem, yu_sem, yd_sem, pc_sem, ts_sem, t_sem,
 ):
@@ -65,7 +74,7 @@
     opp = (t + 2) % NT
 
     loads = [
-        pltpu.make_async_copy(x_hbm.at[pl.ds(pl.multiple_of(t * ROWS, ROWS), ROWS), :], xin, ld_sem.at[0]),
+        pltpu.make_async_copy(x_ref.at[pl.ds(pl.multiple_of(t * ROWS, ROWS), ROWS), :], xin, ld_sem.at[0]),
         pltpu.make_async_copy(wg_hbm, wg, ld_sem.at[1]),
         pltpu.make_async_copy(wu_hbm, wu, ld_sem.at[2]),
         pltpu.make_async_copy(wd_hbm, wd, ld_sem.at[3]),
@@ -218,29 +227,31 @@
         mix_ref[...] = mm(joined, wo[...]).astype(BF)
 
     own = pl.ds(pl.multiple_of(t * ROWS, ROWS), ROWS)
-    r = routes_ref[own, :]
-    r0 = r[:, 0:1]
-    r1 = r[:, 1:2]
-    lane = lax.broadcasted_iota(jnp.int32, (ROWS, NE), 1)
-    s0 = jnp.where(r0 == lane, 1.0, 0.0)
-    s1 = jnp.where(r1 == lane, 1.0, 0.0)
-    low = jnp.where(
-        lax.broadcasted_iota(jnp.int32, (ROWS, ROWS), 0) > lax.broadcasted_iota(jnp.int32, (ROWS, ROWS), 1), 1.0, 0.0
-    )
-    before = mm(low.astype(BF), (s0 + s1).astype(BF))
-    k0 = jnp.sum(before * s0, axis=1, keepdims=True)
-    k1 = jnp.sum((before + s0) * s1, axis=1, keepdims=True)
-    slots = lax.broadcasted_iota(jnp.int32, (ROWS, SL), 1).astype(F32)
-    c0 = jnp.where(r0.astype(F32) * CAP + k0 == slots, 1.0, 0.0)
-    c1 = jnp.where(r1.astype(F32) * CAP + k1 == slots, 1.0, 0.0)
-    pick[0:ROWS, :] = c0.astype(BF)
-    pick[ROWS : 2 * ROWS, :] = c1.astype(BF)
+    tokens = NT * ROWS
+    r = routes_ref[...]
+    r0 = r[0:1, :]
+    r1 = r[1:2, :]
+    expert = lax.broadcasted_iota(jnp.int32, (NE, tokens), 0)
+    s0 = jnp.where(r0 == expert, 1.0, 0.0)
+    s1 = jnp.where(r1 == expert, 1.0, 0.0)
+    ta = lax.broadcasted_iota(jnp.int32, (tokens, tokens), 0)
+    tb = lax.broadcasted_iota(jnp.int32, (tokens, tokens), 1)
+    earlier = jnp.where((ta < tb) & ((ta >> 6) == (tb >> 6)), 1.0, 0.0).astype(BF)
+    before = mm((s0 + s1).astype(BF), earlier)
+    slot0 = r0.astype(F32) * CAP + jnp.sum(before * s0, axis=0, keepdims=True)
+    slot1 = r1.astype(F32) * CAP + jnp.sum((before + s0) * s1, axis=0, keepdims=True)
+
+    slot = lax.broadcasted_iota(jnp.int32, (SL, tokens), 0).astype(F32)
+    pick[0:tokens, :] = jnp.transpose(jnp.where(slot0 == slot, 1.0, 0.0)).astype(BF)
+    pick[tokens : 2 * tokens, :] = jnp.transpose(jnp.where(slot1 == slot, 1.0, 0.0)).astype(BF)
+    wcol[...] = jnp.transpose(jnp.concatenate([rw_ref[...], jnp.zeros((6, tokens), F32)], axis=0))
+    both = jnp.concatenate([pick[own, :], pick[pl.ds(pl.multiple_of(tokens + t * ROWS, ROWS), ROWS), :]], axis=0)
 
     loads[0].wait()
     wide = xin[...].astype(F32)
     scale = lax.rsqrt(jnp.mean(wide * wide, axis=-1, keepdims=True) + 1e-06)
-    normed = (wide * scale * gain_ref[...].astype(F32)).astype(BF)
-    chosen = jnp.transpose(c0 + c1).astype(BF)
+    normed = (wide * scale * gain_ref[...].astype(F32)[None, :]).astype(BF)
+    chosen = jnp.transpose(both[0:ROWS, :].astype(F32) + both[ROWS : 2 * ROWS, :].astype(F32)).astype(BF)
     obuf[...] = mm(chosen, normed).astype(BF)
     for g in range(SL // 16):
         rows_to_tiles(perm, obuf, 16 * g, send, 256 * g)
@@ -248,21 +259,17 @@
     loads[5].wait()
     loads[6].wait()
     pl.semaphore_wait(barrier, NE - 1 + 3)
-    kv_up(0)
-    kv_down(0)
 
     for q in range(NZ):
         far = ((z + DZ[q]) % NZ) * NYC
 
         def ship(j, _, q=q, far=far):
             to = far + (yc + j) % NYC
+            src = send.at[pl.ds(pl.multiple_of(to * CH, CH), CH), :]
+            dst = recv.at[t, pl.ds(pl.multiple_of(q * QR + yc * CH, CH), CH), :]
             pltpu.make_async_remote_copy(
-                src_ref=send.at[pl.ds(pl.multiple_of(to * CH, CH), CH), :],
-                dst_ref=recv.at[t, pl.ds(pl.multiple_of(q * QR + yc * CH, CH), CH), :],
-                send_sem=as_sem,
-                recv_sem=a_sem.at[q],
-                device_id=(to, t),
-                device_id_type=MESH,
+                src_ref=src, dst_ref=dst, send_sem=as_sem, recv_sem=a_sem.at[q],
+                device_id=(to, t), device_id_type=MESH,
             ).start()
             return 0
 
@@ -280,8 +287,9 @@
 
     def arrive(q):
         n = QR - CH if q == 0 else QR
+        dst = recv.at[t, pl.ds(q * QR, n), :]
         pltpu.make_async_remote_copy(
-            src_ref=send.at[pl.ds(0, n), :], dst_ref=recv.at[t, pl.ds(q * QR, n), :],
+            src_ref=dst, dst_ref=dst,
             send_sem=as_sem, recv_sem=a_sem.at[q], device_id=(me, right), device_id_type=MESH,
         ).wait_recv()
 
@@ -313,10 +321,12 @@
     def ways(p):
         return (right, left) if p % 2 == 0 else (left, right)
 
+    first = next(step for step in ORDER if step[0] == "experts")
+
     def experts(p):
         gathered(2 * p)
         gathered(2 * p + 1)
-        if p == 0:
+        if ("experts", p) == first:
             for load in loads[1:4]:
                 load.wait()
         for tt in range(NT):
@@ -368,15 +378,12 @@
         if p == 0:
             back[pl.ds(pl.multiple_of(me * CH, CH), CH), :] = ret[pl.ds(pl.multiple_of(yc * CH, CH), CH), :]
 
-    for step in (
-        (spread, 0), (kv_step, 1), (spread, 1), (relay, 0), (kv_step, 2), (spread, 2), (relay, 1), (kv_step, 3),
-        (spread, 3), (relay, 2), (kv_step, 4), (kv_rows, 0), (experts, 0),
-        (spread, 4), (relay, 3), (kv_rows, 1), (spread, 5), (relay, 4), (kv_rows, 2), (experts, 1), (spread, 6),
-        (relay, 5), (spread, 7), (relay, 6), (relay, 7), (middle, 0), (kv_rows, 3), (attend, 0),
-        (experts, 2), (middle, 1), (finish, 0), (experts, 3), (middle, 2),
-        (finish, 1), (project, 0), (middle, 3), (finish, 2), (finish, 3),
-    ):
-        step[0](step[1])
+    steps = dict(
+        spread=spread, relay=relay, experts=experts, middle=middle, finish=finish, kv=kv_step, rows=kv_rows,
+        attend=attend, project=project,
+    )
+    for name, index in ORDER:
+        steps[name](index)
 
     n = ALL - CH
     last = pltpu.make_async_remote_copy(
@@ -388,8 +395,8 @@
         y = mm(perm, back[256 * g : 256 * g + 256, :]).astype(BF)
         for i in range(TR):
             resb[16 * g : 16 * g + 16, 128 * i : 128 * i + 128] = y[16 * i : 16 * i + 16, :]
-    picked = mm(pick[...], resb[...])
-    w = rw_ref[own, :]
+    picked = mm(both, resb[...])
+    w = wcol[own, :]
     out_ref[...] = (w[:, 0:1] * picked[0:ROWS, :] + w[:, 1:2] * picked[ROWS : 2 * ROWS, :]).astype(BF)
 
     last.wait_send()
@@ -410,7 +417,7 @@
         recv_sem=t_sem.at[0], device_id=(me, right), device_id_type=MESH,
     ).wait_send()
     pltpu.make_async_remote_copy(
-        src_ref=send.at[pl.ds(0, n), :], dst_ref=recv.at[t, pl.ds(0, n), :], send_sem=as_sem, recv_sem=a_sem.at[0],
+        src_ref=send.at[pl.ds(0, n), :], dst_ref=send.at[pl.ds(0, n), :], send_sem=as_sem, recv_sem=a_sem.at[0],
         device_id=(me, right), device_id_type=MESH,
     ).wait_send()
     pltpu.make_async_remote_copy(
@@ -448,7 +455,8 @@
         scratch_shapes=[
             pltpu.VMEM((ROWS, D), BF),
             pltpu.VMEM((SL, D), BF),
-            pltpu.VMEM((2 * ROWS, SL), BF),
+            pltpu.VMEM((2 * NT * ROWS, SL), BF),
+            pltpu.VMEM((NT * ROWS, 8), F32),
             pltpu.VMEM((ALL, 128), BF),
             pltpu.VMEM((NT, ALL, 128), BF),
             pltpu.VMEM((D, HID), BF),
@@ -494,7 +502,7 @@
         cost_estimate=pl.CostEstimate(flops=60_000_000_000, bytes_accessed=8_000_000, transcendentals=0),
         name="layer",
     )(
-        routed_input, routes, route_weight, norm_gain.reshape(1, D),
+        routed_input, routes.T, route_weight.T, norm_gain,
         expert_gate[0], expert_up[0], expert_down[0],
         queries, key_cache[0], value_cache[0], cum_gate, out_weight,
     )

time: 109 us -> 87.1 us (0.80)
  Pallas kernels: 100 us -> 83 us
  local copies, waits for them, and re-layouts: 7.47 us -> 3.24 us
    pallas_call x1, Pallas kernels: 100 us -> 83 us  [body(): pl.pallas_call(layer_kernel, out_shape=(jax.ShapeDtypeStruct((ROWS, D), B...]
    unnamed x4 -> x2, local copies, waits for them, and re-layouts: 6.19 us -> 3.24 us
    reshape x1 -> x0, local copies, waits for them, and re-layouts: 1.28 us -> none  [body(): norm_gain.reshape(1, D)]
where the time goes in v3:
time: 87.1 us; the launch traced here: 86.9 us
  Pallas kernels  83 us (95%)
  local copies, waits for them, and re-layouts  3.24 us (4%)
    pallas_call x1, Pallas kernels, body(): pl.pallas_call(layer_kernel, out_shape=(jax.ShapeDtypeStruct((ROWS, D), B...  83 us
    unnamed x2, local copies, waits for them, and re-layouts  3.24 us

profile of v3, /device:TPU:1, one launch (start us, length us, event | category | flops | bytes accessed | tf_op | source)
XLA Modules:
  0.0 86.9 jit_solution(188395558788415551)
XLA Ops:
  0.6 83.0 %layer.1 = (bf16[64,2048]{1,0:T(8,128)(2,1)}, bf16[32,2048]{1,0:T(8,128)(2,1)}) custom-call(bf16[256,2048]{1,0:T(8,128)(2,1)} %x_ref.1, s32[2,256]{1,0:T(2,128)} %bitcast.12, f32[2,256]{1,0:T(2,128)} %bitcast.13, bf16[2048]{0:T(1024)(128)(2,1)} %gain_ref.1, bf16[2048,256]{1,0:T(8,128)(2,1)} %bitcast.7, bf16[2048,256]{1,0:T(8,128)(2,1)} %bitcast.8, ...), custom_call_target="tpu_custom_call" | custom-call | flops 60000002048 | bytes 8000000 | tf_op jit(solution)/shard_map/layer/pallas_call | solution.py:450
  83.6 1.6 %copy.16 = bf16[32,2048]{1,0:T(8,128)(2,1)} copy(bf16[32,2048]{1,0:T(8,128)(2,1)} %get-tuple-element.8) | data formatting | bytes 262144
  85.2 1.7 %copy.17 = bf16[64,2048]{1,0:T(8,128)(2,1)} copy(bf16[64,2048]{1,0:T(8,128)(2,1)} %get-tuple-element.9) | data formatting | bytes 524288

commit v4 on v3

--- a/solution.py
+++ b/solution.py
@@ -28,15 +28,19 @@
 HEAD = 64
 SEQ = 128
 MIX = SEQ // NT
-DZ = (0, 7, 2, 1, 3, 5, 6, 4)
+DZ = (0, 1, 7, 2, 3, 6, 5, 4)
+ISSUE = (4, 5, 0, 6, 3, 7, 2, 1)
+FULL = tuple(q for q in range(NZ) if DZ[q] in (1, 7))
+PARTS = tuple(q for q in range(NZ) if q not in FULL)
+BLK = NYC * CAP
 ORDER = (
-    ("spread", 0), ("spread", 1), ("relay", 0), ("spread", 2), ("spread", 3), ("spread", 5),
-    ("relay", 1), ("spread", 6), ("spread", 4), ("relay", 2), ("kv", 0), ("relay", 5),
-    ("relay", 4), ("spread", 7), ("relay", 3), ("kv", 1), ("relay", 6), ("kv", 2),
-    ("relay", 7), ("experts", 2), ("kv", 3), ("experts", 3), ("kv", 4), ("rows", 0),
-    ("middle", 2), ("experts", 1), ("middle", 3), ("finish", 2), ("middle", 1), ("rows", 1),
-    ("experts", 0), ("finish", 3), ("rows", 2), ("middle", 0), ("rows", 3), ("finish", 1),
-    ("attend", 0), ("finish", 0), ("project", 0),
+    ("spread", 0), ("spread", 5), ("spread", 4), ("relay", 0), ("relay", 5), ("spread", 3),
+    ("spread", 6), ("relay", 4), ("spread", 7), ("relay", 6), ("relay", 3), ("relay", 7),
+    ("kv", 0), ("experts", 2), ("spread", 2), ("spread", 1), ("kv", 1), ("experts", 3),
+    ("kv", 2), ("kv", 3), ("middle", 2), ("experts", 1), ("kv", 4), ("rows", 0),
+    ("middle", 3), ("finish", 2), ("middle", 1), ("experts", 0), ("rows", 1), ("finish", 3),
+    ("middle", 0), ("rows", 2), ("finish", 1), ("rows", 3), ("attend", 0), ("finish", 0),
+    ("project", 0),
 )
 
 
@@ -59,8 +63,8 @@
 def layer_kernel(
     x_ref, routes_ref, rw_ref, gain_ref, wg_hbm, wu_hbm, wd_hbm, q_ref, key_hbm, value_hbm, gate_ref, wo_hbm,
     out_ref, mix_ref,
-    xin, obuf, pick, wcol, send, recv, wg, wu, wd, xb, part, rs1, rss, rsd, sumb, tot, ret, back, resb, kv, wo, att, att_all,
-    ld_sem, as_sem, a_sem, xs_sem, gl_sem, gr_sem, g2_sem, rr_sem, r1_sem, rss_sem, rsd_sem, bs_sem, b_sem,
+    xin, normed, obuf, pick, wcol, send, sendp, recv, wg, wu, wd, xb, part, rs1, rss, rsd, sumb, tot, ret, back, resb, kv, wo, att, att_all,
+    ld_sem, as_sem, ap_sem, a_sem, xs_sem, gl_sem, gr_sem, g2_sem, rr_sem, r1_sem, rss_sem, rsd_sem, bs_sem, b_sem,
     ks_sem, ku_sem, kd_sem, yu_sem, yd_sem, pc_sem, ts_sem, t_sem,
 ):
     t = lax.axis_index("tp")
@@ -74,7 +78,7 @@
     opp = (t + 2) % NT
 
     loads = [
-        pltpu.make_async_copy(x_ref.at[pl.ds(pl.multiple_of(t * ROWS, ROWS), ROWS), :], xin, ld_sem.at[0]),
+        pltpu.make_async_copy(x_ref, xin, ld_sem.at[0]),
         pltpu.make_async_copy(wg_hbm, wg, ld_sem.at[1]),
         pltpu.make_async_copy(wu_hbm, wu, ld_sem.at[2]),
         pltpu.make_async_copy(wd_hbm, wd, ld_sem.at[3]),
@@ -248,11 +252,15 @@
     both = jnp.concatenate([pick[own, :], pick[pl.ds(pl.multiple_of(tokens + t * ROWS, ROWS), ROWS), :]], axis=0)
 
     loads[0].wait()
-    wide = xin[...].astype(F32)
-    scale = lax.rsqrt(jnp.mean(wide * wide, axis=-1, keepdims=True) + 1e-06)
-    normed = (wide * scale * gain_ref[...].astype(F32)[None, :]).astype(BF)
+
+    def normalise(rows):
+        wide = xin[rows, :].astype(F32)
+        scale = lax.rsqrt(jnp.mean(wide * wide, axis=-1, keepdims=True) + 1e-06)
+        normed[rows, :] = (wide * scale * gain_ref[...].astype(F32)[None, :]).astype(BF)
+
+    normalise(own)
     chosen = jnp.transpose(both[0:ROWS, :].astype(F32) + both[ROWS : 2 * ROWS, :].astype(F32)).astype(BF)
-    obuf[...] = mm(chosen, normed).astype(BF)
+    obuf[...] = mm(chosen, normed[own, :]).astype(BF)
     for g in range(SL // 16):
         rows_to_tiles(perm, obuf, 16 * g, send, 256 * g)
 
@@ -260,21 +268,50 @@
     loads[6].wait()
     pl.semaphore_wait(barrier, NE - 1 + 3)
 
-    for q in range(NZ):
+    sendp4 = sendp.reshape(len(FULL) * NT, QR, 128)
+
+    def dispatch(q):
         far = ((z + DZ[q]) % NZ) * NYC
 
-        def ship(j, _, q=q, far=far):
-            to = far + (yc + j) % NYC
-            src = send.at[pl.ds(pl.multiple_of(to * CH, CH), CH), :]
-            dst = recv.at[t, pl.ds(pl.multiple_of(q * QR + yc * CH, CH), CH), :]
+        def ship(j, _):
+            place = (yc + j) % NYC
+            to = far + place
+            if q in FULL:
+                src = sendp4.at[
+                    pl.ds(FULL.index(q) * NT, NT), pl.ds(pl.multiple_of(place * CH, CH), CH), :
+                ]
+                dst = recv.at[:, pl.ds(pl.multiple_of(q * QR + yc * CH, CH), CH), :]
+            else:
+                src = send.at[pl.ds(pl.multiple_of(to * CH, CH), CH), :]
+                dst = recv.at[t, pl.ds(pl.multiple_of(q * QR + yc * CH, CH), CH), :]
             pltpu.make_async_remote_copy(
-                src_ref=src, dst_ref=dst, send_sem=as_sem, recv_sem=a_sem.at[q],
+                src_ref=src, dst_ref=dst, send_sem=ap_sem if q in FULL else as_sem, recv_sem=a_sem.at[q],
                 device_id=(to, t), device_id_type=MESH,
             ).start()
             return 0
 
         lax.fori_loop(1 if q == 0 else 0, NYC, ship, 0)
+
+    for q in ISSUE:
+        if q not in FULL:
+            dispatch(q)
     recv[t, pl.ds(pl.multiple_of(yc * CH, CH), CH), :] = send[pl.ds(pl.multiple_of(me * CH, CH), CH), :]
+
+    for b in range(NT):
+        normalise(pl.ds(b * ROWS, ROWS))
+    lane = lax.broadcasted_iota(jnp.int32, (BLK, tokens), 1)
+    row = lax.broadcasted_iota(jnp.int32, (BLK, tokens), 0).astype(F32)
+    named = []
+    for q in FULL:
+        goal = row + (((z + DZ[q]) % NZ) * BLK).astype(F32)
+        hit = (slot0 == goal) | (slot1 == goal)
+        named += [jnp.where(hit & ((lane >> 6) == b), 1.0, 0.0) for b in range(NT)]
+    obuf[...] = mm(jnp.concatenate(named, axis=0).astype(BF), normed[...]).astype(BF)
+    for g in range(SL // 16):
+        rows_to_tiles(perm, obuf, 16 * g, sendp, 256 * g)
+    for q in ISSUE:
+        if q in FULL:
+            dispatch(q)
 
     def chunk(src, q):
         return recv.at[src, pl.ds(q * QR, QR), :]
@@ -287,7 +324,7 @@
 
     def arrive(q):
         n = QR - CH if q == 0 else QR
-        dst = recv.at[t, pl.ds(q * QR, n), :]
+        dst = recv.at[:, pl.ds(q * QR, n), :] if q in FULL else recv.at[t, pl.ds(q * QR, n), :]
         pltpu.make_async_remote_copy(
             src_ref=dst, dst_ref=dst,
             send_sem=as_sem, recv_sem=a_sem.at[q], device_id=(me, right), device_id_type=MESH,
@@ -295,11 +332,18 @@
 
     def spread(q):
         arrive(q)
+        if q in FULL:
+            return
         hop(t, q, gl_sem, right).start()
         hop(t, q, gr_sem, left).start()
 
+    def clockwise(q):
+        return PARTS.index(q) % 2 == 0
+
     def relay(q):
-        if q % 2 == 0:
+        if q in FULL:
+            return
+        if clockwise(q):
             hop(left, q, gl_sem, right).wait_recv()
             hop(left, q, g2_sem, right).start()
         else:
@@ -307,7 +351,9 @@
             hop(right, q, g2_sem, left).start()
 
     def gathered(q):
-        if q % 2 == 0:
+        if q in FULL:
+            return
+        if clockwise(q):
             hop(right, q, gr_sem, left).wait_recv()
         else:
             hop(left, q, gl_sem, right).wait_recv()
@@ -416,13 +462,19 @@
         src_ref=att.at[pl.ds(0, 3 * MIX), :], dst_ref=att.at[pl.ds(0, 3 * MIX), :], send_sem=ts_sem,
         recv_sem=t_sem.at[0], device_id=(me, right), device_id_type=MESH,
     ).wait_send()
+    n = len(PARTS) * QR - CH
     pltpu.make_async_remote_copy(
         src_ref=send.at[pl.ds(0, n), :], dst_ref=send.at[pl.ds(0, n), :], send_sem=as_sem, recv_sem=a_sem.at[0],
         device_id=(me, right), device_id_type=MESH,
     ).wait_send()
     pltpu.make_async_remote_copy(
-        src_ref=recv.at[pl.ds(0, 3)], dst_ref=recv.at[pl.ds(0, 3)], send_sem=xs_sem, recv_sem=gl_sem.at[0],
+        src_ref=sendp, dst_ref=sendp, send_sem=ap_sem, recv_sem=a_sem.at[0],
         device_id=(me, right), device_id_type=MESH,
+    ).wait_send()
+    n = len(PARTS) * QR
+    pltpu.make_async_remote_copy(
+        src_ref=recv.at[pl.ds(0, 3), pl.ds(0, n), :], dst_ref=recv.at[pl.ds(0, 3), pl.ds(0, n), :], send_sem=xs_sem,
+        recv_sem=gl_sem.at[0], device_id=(me, right), device_id_type=MESH,
     ).wait_send()
     pltpu.make_async_remote_copy(
         src_ref=part.at[:, pl.ds(0, 3)], dst_ref=part.at[:, pl.ds(0, 3)], send_sem=rr_sem, recv_sem=r1_sem.at[0],
@@ -453,11 +505,13 @@
         in_specs=[hbm, vmem, vmem, vmem, hbm, hbm, hbm, vmem, hbm, hbm, vmem, hbm],
         out_specs=(vmem, vmem),
         scratch_shapes=[
-            pltpu.VMEM((ROWS, D), BF),
+            pltpu.VMEM((NT * ROWS, D), BF),
+            pltpu.VMEM((NT * ROWS, D), BF),
             pltpu.VMEM((SL, D), BF),
             pltpu.VMEM((2 * NT * ROWS, SL), BF),
             pltpu.VMEM((NT * ROWS, 8), F32),
             pltpu.VMEM((ALL, 128), BF),
+            pltpu.VMEM((len(FULL) * NT * QR, 128), BF),
             pltpu.VMEM((NT, ALL, 128), BF),
             pltpu.VMEM((D, HID), BF),
             pltpu.VMEM((D, HID), BF),
@@ -477,6 +531,7 @@
             pltpu.VMEM((SEQ, 2 * HEAD), BF),
             pltpu.VMEM((NT, MIX, 2 * HEAD), BF),
             dma((7,)),
+            dma,
             dma,
             dma((NZ,)),
             dma,

time: 87.1 us -> 82.5 us (0.947)
  Pallas kernels: 83 us -> 78.4 us
    pallas_call x1, Pallas kernels: 83 us -> 78.4 us  [body(): pl.pallas_call(layer_kernel, out_shape=(jax.ShapeDtypeStruct((ROWS, D), B...]
where the time goes in v4:
time: 82.5 us; the launch traced here: 82.3 us
  Pallas kernels  78.4 us (95%)
  local copies, waits for them, and re-layouts  3.24 us (4%)
    pallas_call x1, Pallas kernels, body(): pl.pallas_call(layer_kernel, out_shape=(jax.ShapeDtypeStruct((ROWS, D), B...  78.4 us
    unnamed x2, local copies, waits for them, and re-layouts  3.24 us

profile of v4, /device:TPU:1, one launch (start us, length us, event | category | flops | bytes accessed | tf_op | source)
XLA Modules:
  0.0 82.3 jit_solution(6285178096276433873)
XLA Ops:
  0.6 78.4 %layer.1 = (bf16[64,2048]{1,0:T(8,128)(2,1)}, bf16[32,2048]{1,0:T(8,128)(2,1)}) custom-call(bf16[256,2048]{1,0:T(8,128)(2,1)} %x_ref.1, s32[2,256]{1,0:T(2,128)} %bitcast.12, f32[2,256]{1,0:T(2,128)} %bitcast.13, bf16[2048]{0:T(1024)(128)(2,1)} %gain_ref.1, bf16[2048,256]{1,0:T(8,128)(2,1)} %bitcast.7, bf16[2048,256]{1,0:T(8,128)(2,1)} %bitcast.8, ...), custom_call_target="tpu_custom_call" | custom-call | flops 60000002048 | bytes 8000000 | tf_op jit(solution)/shard_map/layer/pallas_call | solution.py:502
  79.0 1.6 %copy.16 = bf16[32,2048]{1,0:T(8,128)(2,1)} copy(bf16[32,2048]{1,0:T(8,128)(2,1)} %get-tuple-element.8) | data formatting | bytes 262144
  80.6 1.7 %copy.17 = bf16[64,2048]{1,0:T(8,128)(2,1)} copy(bf16[64,2048]{1,0:T(8,128)(2,1)} %get-tuple-element.9) | data formatting | bytes 524288

commit v5 on v4

--- a/solution.py
+++ b/solution.py
@@ -39,7 +39,7 @@
     ("kv", 0), ("experts", 2), ("spread", 2), ("spread", 1), ("kv", 1), ("experts", 3),
     ("kv", 2), ("kv", 3), ("middle", 2), ("experts", 1), ("kv", 4), ("rows", 0),
     ("middle", 3), ("finish", 2), ("middle", 1), ("experts", 0), ("rows", 1), ("finish", 3),
-    ("middle", 0), ("rows", 2), ("finish", 1), ("rows", 3), ("attend", 0), ("finish", 0),
+    ("middle", 0), ("rows", 2), ("finish", 1), ("rows", 3), ("finish", 0), ("attend", 0),
     ("project", 0),
 )
 
@@ -480,6 +480,14 @@
         src_ref=part.at[:, pl.ds(0, 3)], dst_ref=part.at[:, pl.ds(0, 3)], send_sem=rr_sem, recv_sem=r1_sem.at[0],
         device_id=(me, right), device_id_type=MESH,
     ).wait_send()
+
+
+def hand_over(out_ref, mix_ref, out, mix, sems):
+    copies = (pltpu.make_async_copy(out_ref, out, sems.at[0]), pltpu.make_async_copy(mix_ref, mix, sems.at[1]))
+    for copy in copies:
+        copy.start()
+    for copy in copies:
+        copy.wait()
 
 
 def body(
@@ -561,6 +569,15 @@
         expert_gate[0], expert_up[0], expert_down[0],
         queries, key_cache[0], value_cache[0], cum_gate, out_weight,
     )
+    expert_out, mixed_out = pl.pallas_call(
+        hand_over,
+        out_shape=(jax.ShapeDtypeStruct((ROWS, D), BF), jax.ShapeDtypeStruct((MIX, D), BF)),
+        in_specs=[vmem] * 2,
+        out_specs=(hbm, hbm),
+        scratch_shapes=[dma((2,))],
+        compiler_params=pltpu.CompilerParams(vmem_limit_bytes=67043328),
+        name="hand_over",
+    )(expert_out, mixed_out)
     return (mixed_out, expert_out)
 
 

time: 82.5 us -> 80.5 us (0.976)
  local copies, waits for them, and re-layouts: 3.24 us -> 0 us
  Pallas kernels: 78.4 us -> 79.7 us
    unnamed x2 -> x0, local copies, waits for them, and re-layouts: 3.24 us -> none
    pallas_call x0 -> x1, Pallas kernels: none -> 1.74 us  [body(): pl.pallas_call(hand_over, out_shape=(jax.ShapeDtypeStruct((ROWS, D), BF),...]
where the time goes in v5:
time: 80.5 us; the launch traced here: 80.3 us
  Pallas kernels  79.7 us (99%)
    pallas_call x1, Pallas kernels, body(): pl.pallas_call(layer_kernel, out_shape=(jax.ShapeDtypeStruct((ROWS, D), B...  78 us
    pallas_call x1, Pallas kernels, body(): pl.pallas_call(hand_over, out_shape=(jax.ShapeDtypeStruct((ROWS, D), BF),...  1.74 us

profile of v5, /device:TPU:1, one launch (start us, length us, event | category | flops | bytes accessed | tf_op | source)
XLA Modules:
  0.0 80.3 jit_solution(17338951281297200503)
XLA Ops:
  0.6 78.0 %layer.1 = (bf16[64,2048]{1,0:T(8,128)(2,1)}, bf16[32,2048]{1,0:T(8,128)(2,1)}) custom-call(bf16[256,2048]{1,0:T(8,128)(2,1)} %x_ref.1, s32[2,256]{1,0:T(2,128)} %bitcast.12, f32[2,256]{1,0:T(2,128)} %bitcast.13, bf16[2048]{0:T(1024)(128)(2,1)} %gain_ref.1, bf16[2048,256]{1,0:T(8,128)(2,1)} %bitcast.7, bf16[2048,256]{1,0:T(8,128)(2,1)} %bitcast.8, ...), custom_call_target="tpu_custom_call" | custom-call | flops 60000002048 | bytes 8000000 | tf_op jit(solution)/shard_map/layer/pallas_call | solution.py:510
  78.6 1.7 %hand_over.1 = (bf16[64,2048]{1,0:T(8,128)(2,1)}, bf16[32,2048]{1,0:T(8,128)(2,1)}) custom-call(bf16[64,2048]{1,0:T(8,128)(2,1)} %get-tuple-element.6.out_ref, bf16[32,2048]{1,0:T(8,128)(2,1)} %get-tuple-element.7.mix_ref), custom_call_target="tpu_custom_call" | custom-call | tf_op jit(solution)/shard_map/hand_over/pallas_call | solution.py:572

commit v6 on v5

--- a/solution.py
+++ b/solution.py
@@ -403,9 +403,11 @@
         rsend(part.at[p, bwd], rss, rss_sem, p, bwd).wait_recv()
         rsend(sumb.at[p], rsd, rsd_sem, p, fwd).wait_recv()
         tot[...] = (part[p, t].astype(F32) + rss[p].astype(F32) + rsd[p].astype(F32)).astype(BF)
-        for g in range(PT // 16):
-            rows_to_tiles(perm, tot, 16 * g, ret, p * 2 * QR + 256 * g)
+        done = 0
         for q in (2 * p, 2 * p + 1):
+            while done < (q + 1 - 2 * p) * QR:
+                rows_to_tiles(perm, tot, done // TR, ret, p * 2 * QR + done)
+                done += 256
             far = ((z + NZ - DZ[q]) % NZ) * NYC
 
             def home(j, _, q=q, far=far):

time: 80.5 us -> 80.5 us (level)
  no operation moved by 1% of the time
where the time goes in v6:
time: 80.5 us; the launch traced here: 80.3 us
  Pallas kernels  79.7 us (99%)
    pallas_call x1, Pallas kernels, body(): pl.pallas_call(layer_kernel, out_shape=(jax.ShapeDtypeStruct((ROWS, D), B...  77.9 us
    pallas_call x1, Pallas kernels, body(): pl.pallas_call(hand_over, out_shape=(jax.ShapeDtypeStruct((ROWS, D), BF),...  1.74 us

profile of v6, /device:TPU:1, one launch (start us, length us, event | category | flops | bytes accessed | tf_op | source)
XLA Modules:
  0.0 80.3 jit_solution(10892232170555965214)
XLA Ops:
  0.6 77.9 %layer.1 = (bf16[64,2048]{1,0:T(8,128)(2,1)}, bf16[32,2048]{1,0:T(8,128)(2,1)}) custom-call(bf16[256,2048]{1,0:T(8,128)(2,1)} %x_ref.1, s32[2,256]{1,0:T(2,128)} %bitcast.12, f32[2,256]{1,0:T(2,128)} %bitcast.13, bf16[2048]{0:T(1024)(128)(2,1)} %gain_ref.1, bf16[2048,256]{1,0:T(8,128)(2,1)} %bitcast.7, bf16[2048,256]{1,0:T(8,128)(2,1)} %bitcast.8, ...), custom_call_target="tpu_custom_call" | custom-call | flops 60000002048 | bytes 8000000 | tf_op jit(solution)/shard_map/layer/pallas_call | solution.py:512
  78.6 1.7 %hand_over.1 = (bf16[64,2048]{1,0:T(8,128)(2,1)}, bf16[32,2048]{1,0:T(8,128)(2,1)}) custom-call(bf16[64,2048]{1,0:T(8,128)(2,1)} %get-tuple-element.6.out_ref, bf16[32,2048]{1,0:T(8,128)(2,1)} %get-tuple-element.7.mix_ref), custom_call_target="tpu_custom_call" | custom-call | tf_op jit(solution)/shard_map/hand_over/pallas_call | solution.py:574
